TPU v7x, 32 devices: a whole 2x2x4 slice. The times are simulated.
32 devices in a mesh: ep: 8 (over z, x), tp: 4 (over y, core).
Axes of the slice: x: 2, y: 2, z: 4, core: 2. Of those that a mesh axis runs over, the one named last changes fastest.
Arguments:
- mix_in: bfloat16 [1024, 2048], P('ep'), may hold values from -6 to 6
- mix_gain: float32 [2048], replicated, may hold values from 0.1 to 1.9
- query_weight: bfloat16 [2048, 3072], P(None, 'tp'), may hold values from -0.125 to 0.125
- latent_weight: bfloat16 [2048, 512], replicated, may hold values from -0.125 to 0.125
- rotary_weight: bfloat16 [2048, 64], replicated, may hold values from -0.125 to 0.125
- latent_gain: float32 [512], replicated, may hold values from 0.1 to 1.9
- key_weight: bfloat16 [512, 2048], P(None, 'tp'), may hold values from -0.25 to 0.25
- value_weight: bfloat16 [512, 2048], P(None, 'tp'), may hold values from -0.25 to 0.25
- output_weight: bfloat16 [2048, 2048], P('tp'), may hold values from -0.125 to 0.125
- out_gain: float32 [2048], replicated, may hold values from 0.1 to 1.9
- ffn_in: bfloat16 [1024, 2048], P('ep'), may hold values from -6 to 6
- ffn_gain: float32 [2048], replicated, may hold values from 0.1 to 1.9
- gate_weight: bfloat16 [8, 2048, 1024], P('ep', None, 'tp'), may hold values from -0.375 to 0.375
- up_weight: bfloat16 [8, 2048, 1024], P('ep', None, 'tp'), may hold values from -0.375 to 0.375
- down_weight: bfloat16 [8, 1024, 2048], P('ep', 'tp'), may hold values from -0.046875 to 0.046875
- routes: int32 [1024, 4], P('ep'), may hold values from 0 to 7, all different within a row; in each aligned block of 32 rows (0 to 31, 32 to 63, ...) at most 32 rows name the same one
- route_scores: float32 [1024, 4], P('ep'), may hold values from -6 to 6
Outputs:
- mixed: bfloat16 [1024, 2048], P(('ep', 'tp'))
- moe_out: bfloat16 [1024, 2048], P(('ep', 'tp'))
Inputs may be any that keep to these rules, and one draw needn't show every extreme that they name: `routes`: each row names 4 different experts; in each aligned block of 32 rows no expert is named by more than 32 rows, a bound that some blocks reach.
All inputs are finite; a program needn't handle non-finite values.
Results may differ from a plain program's by a relative error of at most 0.014.
Values may be sent and summed in bfloat16 or wider, within the bound.
No kernel may reach another device: no remote copies, remote signals or barrier semaphores. Data moves between devices by JAX's collectives and lax.ppermute only.
A program may use at most 192 MiB of HBM per device.

v0:
```python
import jax
import jax.numpy as jnp
from jax import lax
from jax.sharding import PartitionSpec as P

NOPE = 128
ROPE = 64
VD = 128


norm_eps = 1e-06
clamp_limit = 7.0
gate_slope = 1.702
rope_base = 10000.0


def rms_rows(rows_in, scales):
    mean_square = jnp.mean(rows_in * rows_in, axis=-1, keepdims=True)
    return rows_in * lax.rsqrt(mean_square + norm_eps) * scales


def rms_columns(columns, scales):
    mean_square = jnp.mean(columns * columns, axis=0, keepdims=True)
    return columns * lax.rsqrt(mean_square + norm_eps) * scales[:, None]


def turn_table(positions):
    inverse = rope_base ** (-jnp.arange(0, ROPE, 2).astype(jnp.float32) / ROPE)
    angle_rows = inverse[:, None] * positions.astype(jnp.float32)[None, :]
    return (jnp.cos(angle_rows), jnp.sin(angle_rows))


def clamped_unit(gate_part, linear):
    gate_part = jnp.minimum(gate_part, clamp_limit)
    linear = jnp.clip(linear, -clamp_limit, clamp_limit)
    return gate_part * jax.nn.sigmoid(gate_slope * gate_part) * (linear + 1.0)


def keep_state(running):
    return running


def local(
    mix_in,
    mix_gain,
    query_weight,
    latent_weight,
    rotary_weight,
    latent_gain,
    key_weight,
    value_weight,
    output_weight,
    out_gain,
    ffn_in,
    ffn_gain,
    gate_weight,
    up_weight,
    down_weight,
    routes,
    route_scores,
):
    row_count = mix_in.shape[0]
    first_row = lax.axis_index("ep") * row_count
    last_row = first_row + row_count - 1
    positions = first_row + jnp.arange(row_count, dtype=jnp.int32)
    normed = rms_rows(mix_in.astype(jnp.float32), mix_gain).astype(jnp.bfloat16)
    head_count = query_weight.shape[1] // (NOPE + ROPE)
    half_rope = ROPE // 2
    cosine, sine_rows = turn_table(positions)
    queries = jnp.dot(normed, query_weight, preferred_element_type=jnp.float32).reshape(
        row_count, head_count, NOPE + ROPE
    )
    query_plain = queries[..., :NOPE].astype(jnp.bfloat16)
    query_cos = cosine.T[:, None, :]
    query_sin = sine_rows.T[:, None, :]
    query_upper = queries[..., NOPE : NOPE + half_rope]
    query_lower = queries[..., NOPE + half_rope :]
    query_turn = jnp.concatenate(
        [
            query_upper * query_cos - query_lower * query_sin,
            query_lower * query_cos + query_upper * query_sin,
        ],
        axis=-1,
    ).astype(jnp.bfloat16)
    across = (((0,), (1,)), ((), ()))
    latent = rms_columns(
        lax.dot_general(latent_weight, normed, across, preferred_element_type=jnp.float32),
        latent_gain,
    ).astype(jnp.bfloat16)
    rot_raw = lax.dot_general(rotary_weight, normed, across, preferred_element_type=jnp.float32)
    rotary_key = jnp.concatenate(
        [
            rot_raw[:half_rope] * cosine - rot_raw[half_rope:] * sine_rows,
            rot_raw[half_rope:] * cosine + rot_raw[:half_rope] * sine_rows,
        ],
        axis=0,
    ).astype(jnp.bfloat16)
    score_scale = (NOPE + ROPE) ** (-0.5)
    contract_first = (((0,), (0,)), ((), ()))

    def expand(latent_block):
        key_block = lax.dot_general(
            key_weight, latent_block, contract_first, preferred_element_type=jnp.float32
        ).astype(jnp.bfloat16)
        value_block = lax.dot_general(
            value_weight, latent_block, contract_first, preferred_element_type=jnp.float32
        ).astype(jnp.bfloat16)
        return (key_block, value_block)

    def attend(key_block, value_block, turn_block):
        key_count = key_block.shape[1]
        key_block = key_block.reshape(head_count, NOPE, key_count)
        value_block = value_block.reshape(head_count, VD, key_count)
        scores = jnp.einsum(
            "ihd,hdj->hij", query_plain, key_block, preferred_element_type=jnp.float32
        )
        scores = scores + jnp.einsum(
            "ihd,dj->hij", query_turn, turn_block, preferred_element_type=jnp.float32
        )
        key_places = jnp.arange(key_count, dtype=jnp.int32)
        allowed = key_places[None, :] <= positions[:, None]
        weights = jnp.where(allowed[None], jnp.exp(scores * score_scale), 0.0)
        weighted = jnp.einsum(
            "hij,hdj->hid",
            weights.astype(jnp.bfloat16),
            value_block,
            preferred_element_type=jnp.float32,
        )
        return (jnp.sum(weights, axis=-1), weighted)

    initial = (
        jnp.zeros((head_count, row_count), jnp.float32),
        jnp.zeros((head_count, row_count, VD), jnp.float32),
    )
    shard_piece = (
        lax.all_gather(latent, "ep", axis=1, tiled=True),
        lax.all_gather(rotary_key, "ep", axis=1, tiled=True),
    )

    def compute_piece(running):
        key_block, value_block = expand(shard_piece[0])
        return attend(key_block, value_block, shard_piece[1])

    totals, weighted = lax.cond(jnp.int32(0) > last_row, keep_state, compute_piece, initial)
    attended = (weighted / totals[..., None]).astype(jnp.bfloat16)
    mixing = output_weight.reshape(head_count, VD, output_weight.shape[1])
    partial_value = jnp.einsum("hid,hde->ie", attended, mixing, preferred_element_type=jnp.float32)
    projected = lax.psum_scatter(
        lax.optimization_barrier(partial_value.astype(jnp.bfloat16))
        .astype(jnp.float32)
        .astype(jnp.bfloat16),
        "tp",
        scatter_dimension=0,
        tiled=True,
    ).astype(jnp.float32)
    mixed = rms_rows(projected, out_gain).astype(jnp.bfloat16)
    tokens = ffn_in.shape[0]
    part_count = lax.axis_size("tp")
    quarter_rows = tokens // part_count
    experts = lax.axis_size("ep")
    choose = routes.shape[1]
    capacity = max(2, 2 * quarter_rows * choose // experts)
    slot_count = capacity * part_count
    tp_index = lax.axis_index("tp")
    normed_b = rms_rows(ffn_in.astype(jnp.float32), ffn_gain).astype(jnp.bfloat16)
    padded = jnp.concatenate([normed_b, jnp.zeros((1, normed_b.shape[1]), jnp.bfloat16)], axis=0)
    gate_share = jax.nn.softmax(route_scores, axis=-1)
    grouped = routes.reshape(part_count, quarter_rows * choose)
    onehot = (grouped[:, :, None] == jnp.arange(experts, dtype=jnp.int32)[None, None, :]).astype(
        jnp.int32
    )
    slot_rank = jnp.sum((jnp.cumsum(onehot, axis=1) - 1) * onehot, axis=2)
    slot_index = jnp.arange(part_count, dtype=jnp.int32)[:, None] * capacity + slot_rank
    place_index = (slot_index * experts + grouped).reshape(-1)
    owners = jnp.arange(tokens * choose, dtype=jnp.int32) // choose
    slot_token = jnp.full((slot_count * experts,), tokens, jnp.int32).at[place_index].set(owners)
    unit_count = gate_weight.shape[2]
    chosen = lax.dynamic_slice_in_dim(
        slot_token, tp_index * capacity * experts, capacity * experts, 0
    )
    outgoing = padded[chosen].reshape(capacity, experts, -1)
    arrived = lax.all_to_all(outgoing, "ep", split_axis=1, concat_axis=1, tiled=True)
    row_block = lax.all_gather(arrived, "tp", axis=0, tiled=True)
    block_slots = row_block.shape[0]
    flat_rows = row_block.reshape(-1, row_block.shape[2])
    gate_part = jnp.dot(flat_rows, gate_weight[0], preferred_element_type=jnp.float32)
    up_part = jnp.dot(flat_rows, up_weight[0], preferred_element_type=jnp.float32)
    hidden = (
        clamped_unit(gate_part, up_part).astype(jnp.bfloat16).reshape(block_slots, -1, unit_count)
    )
    sources = hidden.shape[1]
    hidden_flat = hidden.reshape(slot_count * sources, unit_count)
    partial_value = jnp.dot(hidden_flat, down_weight[0], preferred_element_type=jnp.float32)
    result = lax.psum_scatter(
        lax.optimization_barrier(partial_value.astype(jnp.bfloat16))
        .astype(jnp.float32)
        .astype(jnp.bfloat16),
        "tp",
        scatter_dimension=0,
        tiled=True,
    )
    result = result.reshape(capacity, sources, -1)
    returned = lax.all_to_all(result, "ep", split_axis=1, concat_axis=1, tiled=True)
    back_rows = returned.reshape(capacity * experts, -1)
    own_rank = lax.dynamic_index_in_dim(slot_rank, tp_index, 0, keepdims=False)
    own_expert = lax.dynamic_index_in_dim(grouped, tp_index, 0, keepdims=False)
    picked = (
        back_rows[own_rank * experts + own_expert]
        .astype(jnp.float32)
        .reshape(quarter_rows, choose, -1)
    )
    own_gates = lax.dynamic_slice_in_dim(gate_share, tp_index * quarter_rows, quarter_rows, 0)
    moe_out = jnp.sum(picked * own_gates[:, :, None], axis=1).astype(jnp.bfloat16)
    return (mixed, moe_out)


def solution(mesh):
    placed = (
        P("ep", None),
        P(),
        P(None, "tp"),
        P(),
        P(),
        P(),
        P(None, "tp"),
        P(None, "tp"),
        P("tp", None),
        P(),
        P("ep", None),
        P(),
        P("ep", None, "tp"),
        P("ep", None, "tp"),
        P("ep", "tp", None),
        P("ep", None),
        P("ep", None),
    )
    return jax.shard_map(
        local,
        mesh=mesh,
        in_specs=placed,
        out_specs=(P(("ep", "tp"), None), P(("ep", "tp"), None)),
        check_vma=False,
    )
```

profile of v0, /device:TPU:0, one launch (start us, length us, event | category | flops | bytes accessed | tf_op | source)
XLA Modules:
  0.0 232.8 jit_solution(3613812320336969351)
XLA Ops:
  10.8 2.5 %scatter_custom_fusion = s32[1024]{0:T(1024)S(1)} fusion(s32[512]{0:T(512)S(1)} %bitcast.86, s32[512]{0:T(512)S(1)} %add_select_fusion, s32[]{:T(128)} %constant.36.clone.1), kind=kCustom, calls=%fused_computation.95 | custom fusion | bytes 4100 | tf_op jit(solution)/shard_map/scatter | solution.py:176
  16.7 4.5 %gather_fusion = bf16[256,2048]{1,0:T(8,128)(2,1)} fusion(bf16[129,2048]{1,0:T(8,128)(2,1)} %concatenate.13, s32[1024]{0:T(1024)S(1)} %pad_clamp_fusion.1), kind=kCustom, calls=%fused_computation | custom fusion | bytes 2098176 | tf_op jit(solution)/shard_map/gather | solution.py:181
  21.2 1.8 copy.43
  23.0 32.8 %all_to_all.10 = bf16[32,8,2048]{2,0,1:T(8,128)(2,1)S(1)} all-to-all(bf16[32,8,2048]{2,0,1:T(8,128)(2,1)S(1)} %copy.43), channel_id=1, replica_groups=mesh['ep'=8,'tp'=4] {'ep'}, dimensions={1} | all-to-all | bytes 2097152 | tf_op jit(solution)/shard_map/all_to_all | solution.py:182
  58.7 2.3 %multiply_reduce_fusion.1 = (f32[128]{0:T(128)S(1)}, f32[128,512]{1,0:T(8,128)S(1)}) fusion(bf16[2048,512]{1,0:T(8,128)(2,1)} %param.22, bf16[128,2048]{1,0:T(8,128)(2,1)} %param.19, f32[2048]{0:T(1024)S(1)} %copy-done.4, f32[128]{0:T(128)S(1)} %add_rsqrt_fusion.3), kind=kOutput, calls=%fused_computation.63 | convolution fusion | flops 269614976 | bytes 2892800 | tf_op jit(solution)/shard_map/dot_general | solution.py:87
  61.9 29.2 %all-gather.5.cloned.1.call-done = bf16[128,8,2048]{2,1,0:T(8,128)(2,1)} async-done(((bf16[32,8,2048]{2,1,0:T(8,128)(2,1)}), bf16[128,8,2048]{2,1,0:T(8,128)(2,1)}) %all-gather.5.cloned.1.call-update) | async-done | bytes 4194320 | tf_op jit(solution)/shard_map/all_gather | solution.py:183
  91.1 4.7 %fusion.12 = f32[1024,256]{1,0:T(8,128)} fusion(bf16[128,8,2048]{2,1,0:T(8,128)(2,1)} %all-gather.5.cloned.1.call-done, bf16[1,2048,256]{2,1,0:T(8,128)(2,1)} %param.31), kind=kOutput, calls=%fused_computation.22 | convolution fusion | flops 1074003968 | bytes 6291456 | tf_op jit(solution)/shard_map/dot_general | solution.py:186
  95.8 9.4 %convolution_convert_fusion.2 = bf16[1024,2048]{1,0:T(8,128)(2,1)} fusion(bf16[128,8,2048]{2,1,0:T(8,128)(2,1)} %all-gather.5.cloned.1.call-done, bf16[1,256,2048]{2,1,0:T(8,128)(2,1)} %param.33, bf16[1,2048,256]{2,1,0:T(8,128)(2,1)} %param.32, f32[1024,256]{1,0:T(8,128)} %fusion.12), kind=kOutput, calls=%fused_computation.19 | convolution fusion | flops 2151940096 | bytes 11534336 | tf_op jit(solution)/shard_map/dot_general | solution.py:193
  107.7 27.7 %all_gather.10 = bf16[64,1024]{1,0:T(8,128)(2,1)} all-gather(bf16[64,128]{1,0:T(8,128)(2,1)S(1)} %pad_maximum_fusion.1), channel_id=1, replica_groups=mesh['ep'=8,'tp'=4] {'ep'}, dimensions={1}, use_global_device_ids=true | all-gather | bytes 147456 | tf_op jit(solution)/shard_map/all_gather | solution.py:137
  136.1 2.4 %fusion.79 = f32[128,768]{0,1:T(8,128)S(1)} fusion(bf16[2048,768]{1,0:T(8,128)(2,1)S(1)} %copy-done, bf16[128,2048]{1,0:T(8,128)(2,1)} %param.19, f32[2048]{0:T(1024)S(1)} %copy-done.4, f32[128]{0:T(128)} %copy-done.7), kind=kOutput, calls=%fused_computation.118 | convolution fusion | flops 403701760 | bytes 4071936 | tf_op jit(solution)/shard_map/dot_general | solution.py:70
  139.2 8.9 %conditional.1 = (f32[4,128]{1,0:T(4,128)S(1)}, f32[4,128,128]{2,1,0:T(8,128)S(1)}) conditional(s32[]{:T(128)} %convert_element_type.84, (s32[128]{0:T(128)}, bf16[512,512]{1,0:T(8,128)(2,1)}, bf16[512,1024]{0,1:T(8,128)(2,1)}, f32[128,4,192]{0,2,1:T(8,128)S(1)}, bf16[64,1024]{1,0:T(8,128)(2,1)}, /*index=5*/bf16[128,4,64]{0,2,1:T(8,128)(2,1)}, ...), branch_computations={%region_2.4_spmd, %region_4.5_spmd} | conditional | flops 1413086720 | bytes 22155932 | solution.py:144
  139.2 3.2 %convolution_convert_fusion.1 = bf16[512,1024]{1,0:T(8,128)(2,1)} fusion(bf16[512,512]{1,0:T(8,128)(2,1)} %get-tuple-element.30, bf16[512,1024]{0,1:T(8,128)(2,1)} %get-tuple-element.49), kind=kOutput, calls=%fused_computation.8 | convolution fusion | flops 537395200 | bytes 2621440 | tf_op jit(solution)/shard_map/cond/branch_0_fun/dot_general | solution.py:102
  143.2 2.1 fusion.5
  148.1 2.9 %fusion.11 = bf16[128,2048]{1,0:T(8,128)(2,1)} fusion(bf16[4,128,2048]{2,1,0:T(8,128)(2,1)} %bitcast.81, f32[4,128,128]{2,1,0:T(8,128)S(1)} %get-tuple-element.25, f32[4,128]{1,0:T(4,128)S(1)} %get-tuple-element.26), kind=kOutput, calls=%fused_computation.21 | convolution fusion | flops 268828672 | bytes 2885632 | tf_op jit(solution)/shard_map/hid,hde->ie/dot_general | solution.py:147
  151.0 29.7 %reduce-scatter.5.cloned.1.call-done = bf16[256,2048]{1,0:T(8,128)(2,1)} async-done(((bf16[1024,2048]{1,0:T(8,128)(2,1)}), bf16[256,2048]{1,0:T(8,128)(2,1)}) %reduce-scatter.5.cloned.1.call-update) | async-done | bytes 1048592 | tf_op jit(solution)/shard_map/reduce_scatter | solution.py:194
  180.7 2.9 %copy.45 = bf16[32,8,2048]{2,0,1:T(8,128)(2,1)} copy(bf16[32,8,2048]{2,1,0:T(8,128)(2,1)} %bitcast.83) | data formatting | bytes 2097152 | tf_op jit(solution)/shard_map/reshape | solution.py:202
  183.6 5.5 %all-to-all-start.1 = ((bf16[32,8,2048]{2,0,1:T(8,128)(2,1)}), bf16[32,8,2048]{2,0,1:T(8,128)(2,1)}, u32[]{:S(2)}, u32[]{:S(2)}) async-start(bf16[32,8,2048]{2,0,1:T(8,128)(2,1)} %copy.45), calls=%async_computation.3 | async-start | bytes 2097152 | tf_op jit(solution)/shard_map/all_to_all | solution.py:203
  189.4 15.4 %reduce-scatter.3.cloned.1.call-done = bf16[32,2048]{1,0:T(8,128)(2,1)} async-done(((bf16[128,2048]{1,0:T(8,128)(2,1)}), bf16[32,2048]{1,0:T(8,128)(2,1)}) %reduce-scatter.3.cloned.1.call-update) | async-done | bytes 131088 | tf_op jit(solution)/shard_map/reduce_scatter | solution.py:148
  205.8 1.7 fusion.51
  207.5 7.4 %all-to-all-done.1 = bf16[32,8,2048]{2,0,1:T(8,128)(2,1)} async-done(((bf16[32,8,2048]{2,0,1:T(8,128)(2,1)}), bf16[32,8,2048]{2,0,1:T(8,128)(2,1)}, u32[]{:S(2)}, u32[]{:S(2)}) %all-to-all-start.1) | async-done | bytes 1048608 | tf_op jit(solution)/shard_map/all_to_all | solution.py:203
  214.9 2.8 %copy.53 = bf16[32,8,2048]{2,1,0:T(8,128)(2,1)} copy(bf16[32,8,2048]{2,0,1:T(8,128)(2,1)} %all-to-all-done.1) | data formatting | bytes 2097152 | tf_op jit(solution)/shard_map/all_to_all | solution.py:203
  217.7 3.6 %gather_fusion.1 = bf16[128,2048]{1,0:T(8,128)(2,1)} fusion(bf16[256,2048]{1,0:T(8,128)(2,1)} %bitcast.77, s32[1024]{0:T(1024)S(1)} %pad_clamp_fusion), kind=kCustom, calls=%fused_computation.1 | custom fusion | bytes 1049088 | tf_op jit(solution)/shard_map/gather | solution.py:208
  221.3 2.4 %reshape.248 = f32[32,4,2048]{2,1,0:T(4,128)} reshape(bf16[128,2048]{1,0:T(8,128)(2,1)} %gather_fusion.1) | data formatting | bytes 1572864 | tf_op jit(solution)/shard_map/convert_element_type | solution.py:209
  223.7 2.6 %multiply_reduce_fusion = bf16[32,2048]{1,0:T(8,128)(2,1)} fusion(f32[32,4,2048]{2,1,0:T(4,128)} %reshape.248, f32[32,4]{1,0:T(8,128)S(1)} %copy.47), kind=kLoop, calls=%fused_computation.42 | loop fusion | flops 458752 | bytes 1180160 | tf_op jit(solution)/shard_map/reduce_sum | solution.py:213
  (77 shorter events, 19.4 us)
Async XLA Ops:
  7.2 128.9 %copy-start = (bf16[2048,768]{1,0:T(8,128)(2,1)S(1)}, bf16[2048,768]{1,0:T(8,128)(2,1)}, u32[]{:S(2)}) copy-start(bf16[2048,768]{1,0:T(8,128)(2,1)} %param.21) | copy-start | bytes 9437188
  7.2 83.9 %all-gather.5.cloned.1.call-start = ((), (), s32[]{:S(2)}) async-start(), calls=%async_computation.6 | async-start | bytes 5242880 | tf_op jit(solution)/shard_map/all_gather | solution.py:183
  55.8 2.9 %copy-start.4 = (f32[2048]{0:T(1024)S(1)}, f32[2048]{0:T(1024)}, u32[]{:S(2)}) copy-start(f32[2048]{0:T(1024)} %param.20) | copy-start | bytes 24580
  57.4 3.7 %copy-start.6 = (f32[512]{0:T(512)S(1)}, f32[512]{0:T(512)}, u32[]{:S(2)}) copy-start(f32[512]{0:T(512)} %param.24) | copy-start | bytes 6148
  57.4 81.8 %all-gather.3.cloned.1.call-start = ((), (), s32[]{:S(2)}) async-start(), calls=%async_computation.4 | async-start | bytes 1179648 | tf_op jit(solution)/shard_map/all_gather | solution.py:136
  58.7 46.6 %copy-start.7 = (f32[128]{0:T(128)}, f32[128]{0:T(128)S(1)}, u32[]{:S(2)}) copy-start(f32[128]{0:T(128)S(1)} %add_rsqrt_fusion.3) | copy-start | bytes 1540
  61.8 118.9 %reduce-scatter.5.cloned.1.call-start = ((), (), s32[]{:S(2)}) async-start(), calls=%async_computation.7 | async-start | bytes 5242880 | tf_op jit(solution)/shard_map/reduce_scatter | solution.py:194
  105.2 0.9 copy-start.11
  105.2 99.6 %reduce-scatter.3.cloned.1.call-start = ((), (), s32[]{:S(2)}) async-start(), calls=%async_computation.5 | async-start | bytes 655360 | tf_op jit(solution)/shard_map/reduce_scatter | solution.py:148
  142.4 3.0 %copy-start.8 = (s32[128]{0:T(128)S(1)}, s32[128]{0:T(128)}, u32[]{:S(2)}) copy-start(s32[128]{0:T(128)} %get-tuple-element.14) | copy-start | bytes 1540 | tf_op jit(solution)/shard_map/cond
  143.2 2.3 copy-start.1
  143.2 2.3 copy-start.2
  145.3 1.3 copy-start.9
  145.4 1.5 copy-start.10
  180.7 8.4 %copy-start.3 = (f32[128,4]{0,1:T(4,128)S(1)}, f32[128,4]{0,1:T(4,128)}, u32[]{:S(2)}) copy-start(f32[128,4]{0,1:T(4,128)} %param.35) | copy-start | bytes 6148
  180.7 25.1 %copy-start.5 = (f32[2048]{0:T(1024)S(1)}, f32[2048]{0:T(1024)}, u32[]{:S(2)}) copy-start(f32[2048]{0:T(1024)} %param.28) | copy-start | bytes 24580
  183.6 31.3 %all-to-all-start.1 = ((bf16[32,8,2048]{2,0,1:T(8,128)(2,1)}), bf16[32,8,2048]{2,0,1:T(8,128)(2,1)}, u32[]{:S(2)}, u32[]{:S(2)}) async-start(bf16[32,8,2048]{2,0,1:T(8,128)(2,1)} %copy.45), calls=%async_computation.3 | async-start | bytes 2097152 | tf_op jit(solution)/shard_map/all_to_all | solution.py:203
Sparse Core Ops, SparseCore 0:
  57.5 33.4 all-gather.4
  93.8 40.4 all-gather.2
  136.8 43.9 reduce-scatter.4
  183.1 21.6 reduce-scatter.2
where the time goes:
time: 234 us; the launch traced here: 233 us
  waiting for transfers between devices  81.7 us (35%)
  blocking collectives  60.5 us (26%)
  matrix products  30.5 us (13%)
  local copies, waits for them, and re-layouts  26.4 us (11%)
  between operations  14 us (6%)
  other arithmetic  13.9 us (6%)
  starting transfers between devices  5.68 us (2%)
    reduce_scatter x2, waiting for transfers between devices, local(): lax.psum_scatter(lax.optimization_barrier(partial_value.astype(jnp.bfloat...  45.1 us
    all_to_all x1, blocking collectives, local(): lax.all_to_all(outgoing, 'ep', split_axis=1, concat_axis=1, tiled=True)  32.8 us
    all_gather x1, waiting for transfers between devices, local(): row_block = lax.all_gather(arrived, 'tp', axis=0, tiled=True)  29.2 us
    all_gather x1, blocking collectives, local(): lax.all_gather(rotary_key, 'ep', axis=1, tiled=True)  27.7 us
    dot_general x1, matrix products, local(): jnp.dot(hidden_flat, down_weight[0], preferred_element_type=jnp.float32)  9.41 us
    all_to_all x1, waiting for transfers between devices, local(): lax.all_to_all(result, 'ep', split_axis=1, concat_axis=1, tiled=True)  7.37 us
    all_to_all x1, starting transfers between devices, local(): lax.all_to_all(result, 'ep', split_axis=1, concat_axis=1, tiled=True)  5.52 us
    dot_general x1, matrix products, local(): jnp.dot(flat_rows, gate_weight[0], preferred_element_type=jnp.float32)  4.72 us
  transfers between devices with their start and end apart: 5, of which 4 were waited for; matrix products, arithmetic and copies ran while one was open for 18% of the time, Pallas kernels for 0%

commit v1 on v0

--- a/solution.py
+++ b/solution.py
@@ -1,6 +1,8 @@
 import jax
 import jax.numpy as jnp
 from jax import lax
+from jax.experimental import pallas as pl
+from jax.experimental.pallas import tpu as pltpu
 from jax.sharding import PartitionSpec as P
 
 NOPE = 128
@@ -40,7 +42,7 @@
     return running
 
 
-def local(
+def local_routed(
     mix_in,
     mix_gain,
     query_weight,
@@ -213,6 +215,237 @@
     moe_out = jnp.sum(picked * own_gates[:, :, None], axis=1).astype(jnp.bfloat16)
     return (mixed, moe_out)
 
+LANES = 128
+
+
+def turn_rows(rows, cosine, sine_rows):
+    half_rope = ROPE // 2
+    upper = rows[..., :half_rope]
+    lower = rows[..., half_rope:]
+    return jnp.concatenate(
+        [upper * cosine - lower * sine_rows, lower * cosine + upper * sine_rows], axis=-1
+    )
+
+
+def expert_rows(expert_ref, rows_ref, side_ref, gate_ref, up_ref, down_ref, out_ref, *, experts):
+    rows = rows_ref[...]
+    gate_part = jnp.dot(rows, gate_ref[...], preferred_element_type=jnp.float32)
+    up_part = jnp.dot(rows, up_ref[...], preferred_element_type=jnp.float32)
+    hidden = clamped_unit(gate_part, up_part).astype(jnp.bfloat16)
+    result = jnp.dot(hidden, down_ref[...], preferred_element_type=jnp.float32)
+    column = lax.broadcasted_iota(jnp.int32, side_ref.shape, 1) - ROPE
+    mine = (column == expert_ref[0]) | (column == expert_ref[0] + experts)
+    share = jnp.sum(
+        jnp.where(mine, side_ref[...].astype(jnp.float32), 0.0), axis=1, keepdims=True
+    )
+    out_ref[...] = (result * share).astype(jnp.bfloat16)
+
+
+def apply_expert(expert, block, gate_w, up_w, down_w, latent_width, experts):
+    count = block.shape[0]
+    width = gate_w.shape[0]
+    units = gate_w.shape[1]
+    step = min(256, count)
+    side_width = block.shape[1] - width - latent_width
+    whole = lambda i: (0, 0)
+    return pl.pallas_call(
+        lambda *refs: expert_rows(*refs, experts=experts),
+        grid=(count // step,),
+        in_specs=[
+            pl.BlockSpec(memory_space=pltpu.SMEM),
+            pl.BlockSpec((step, width), lambda i: (i, 0)),
+            pl.BlockSpec((step, side_width), lambda i: (i, (width + latent_width) // side_width)),
+            pl.BlockSpec((width, units), whole),
+            pl.BlockSpec((width, units), whole),
+            pl.BlockSpec((units, width), whole),
+        ],
+        out_specs=pl.BlockSpec((step, width), lambda i: (i, 0)),
+        out_shape=jax.ShapeDtypeStruct((count, width), jnp.bfloat16),
+        cost_estimate=pl.CostEstimate(
+            flops=6 * count * width * units,
+            bytes_accessed=4 * count * width + 6 * width * units,
+            transcendentals=count * units,
+        ),
+        name="expert_rows",
+    )(expert, block, block, gate_w, up_w, down_w)
+
+
+def add_pieces(left, right):
+    return (left.astype(jnp.float32) + right.astype(jnp.float32)).astype(jnp.bfloat16)
+
+
+def local_dense(
+    mix_in,
+    mix_gain,
+    query_weight,
+    latent_weight,
+    rotary_weight,
+    latent_gain,
+    key_weight,
+    value_weight,
+    output_weight,
+    out_gain,
+    ffn_in,
+    ffn_gain,
+    gate_weight,
+    up_weight,
+    down_weight,
+    routes,
+    route_scores,
+):
+    row_count, width = mix_in.shape
+    ep_size = lax.axis_size("ep")
+    tp_size = lax.axis_size("tp")
+    experts = ep_size
+    lines = ep_size // 2
+    piece = row_count // tp_size
+    ep_index = lax.axis_index("ep")
+    tp_index = lax.axis_index("tp")
+    latent_width = latent_weight.shape[1]
+    head_count = query_weight.shape[1] // (NOPE + ROPE)
+
+    def swap(array, axis, bit):
+        size = ep_size if axis == "ep" else tp_size
+        return lax.ppermute(array, axis, [(i, i ^ bit) for i in range(size)])
+
+    own_rows = lax.dynamic_slice_in_dim(ffn_in, tp_index * piece, piece, 0)
+    own_routes = lax.dynamic_slice_in_dim(routes, tp_index * piece, piece, 0)
+    own_scores = lax.dynamic_slice_in_dim(route_scores, tp_index * piece, piece, 0)
+    own_mix = lax.dynamic_slice_in_dim(mix_in, tp_index * piece, piece, 0)
+    normed_b = rms_rows(own_rows.astype(jnp.float32), ffn_gain).astype(jnp.bfloat16)
+    gate_share = jax.nn.softmax(own_scores, axis=-1)
+    named = own_routes[:, :, None] == jnp.arange(experts, dtype=jnp.int32)[None, None, :]
+    shares = jnp.sum(jnp.where(named, gate_share[:, :, None], 0.0), axis=1)
+    shares_high = lax.reduce_precision(shares, 8, 7)
+    shares_low = shares - shares_high
+    own_first = ep_index * row_count + tp_index * piece
+    own_cos, own_sin = turn_table(own_first + jnp.arange(piece, dtype=jnp.int32))
+    own_normed = rms_rows(own_mix.astype(jnp.float32), mix_gain).astype(jnp.bfloat16)
+    latent = rms_rows(
+        jnp.dot(own_normed, latent_weight, preferred_element_type=jnp.float32), latent_gain
+    ).astype(jnp.bfloat16)
+    rotary_key = turn_rows(
+        jnp.dot(own_normed, rotary_weight, preferred_element_type=jnp.float32),
+        own_cos.T,
+        own_sin.T,
+    ).astype(jnp.bfloat16)
+    used = ROPE + 2 * experts
+    side = jnp.concatenate(
+        [
+            rotary_key,
+            shares_high.astype(jnp.bfloat16),
+            shares_low.astype(jnp.bfloat16),
+            jnp.zeros((piece, -used % LANES), jnp.bfloat16),
+        ],
+        axis=1,
+    )
+    own = jnp.concatenate([normed_b, latent, side], axis=1)[None]
+
+    line = jnp.concatenate([own] + [swap(own, "ep", 2 * k) for k in range(1, lines)], axis=0)
+    from_x = swap(line, "ep", 1)
+    from_y = swap(line, "tp", 2)
+    half = lines // 2
+    diagonal = [swap(from_y[:half], "ep", 1), swap(from_x[half:], "tp", 2)]
+    near = jnp.concatenate([line, from_y, from_x] + diagonal, axis=0)
+    near = near.reshape(4 * lines * piece, -1)
+    far = swap(near, "tp", 1)
+
+    expert = ep_index.astype(jnp.int32).reshape(1)
+    weights_of = (gate_weight[0], up_weight[0], down_weight[0])
+    near_out = apply_expert(expert, near, *weights_of, latent_width, experts)
+    far_out = apply_expert(expert, far, *weights_of, latent_width, experts)
+
+    blocks = add_pieces(near_out, swap(far_out, "tp", 1)).reshape(4, lines, piece, width)
+    got_x = swap(blocks[2:, :half], "ep", 1)
+    got_y = swap(blocks[1::2, half:], "tp", 2)
+    first = add_pieces(blocks[:2, :half], got_x)
+    second = add_pieces(blocks[0::2, half:], got_y)
+    got_y = swap(first[1], "tp", 2)
+    got_x = swap(second[1], "ep", 1)
+    summed = jnp.concatenate(
+        [add_pieces(first[0], got_y), add_pieces(second[0], got_x)], axis=0
+    )
+    moe_sum = summed[0].astype(jnp.float32)
+    for k in range(1, lines):
+        moe_sum = moe_sum + swap(summed[k], "ep", 2 * k).astype(jnp.float32)
+    moe_out = moe_sum.astype(jnp.bfloat16)
+
+    order = tp_index ^ jnp.arange(tp_size, dtype=jnp.int32)
+    mix_rows = jnp.concatenate(
+        [
+            lax.dynamic_slice_in_dim(mix_in, (tp_index ^ k) * piece, piece, 0)
+            for k in range(tp_size)
+        ],
+        axis=0,
+    )
+    steps = jnp.arange(piece, dtype=jnp.int32)
+    positions = (ep_index * row_count + order[:, None] * piece + steps[None, :]).reshape(-1)
+    normed = rms_rows(mix_rows.astype(jnp.float32), mix_gain).astype(jnp.bfloat16)
+    cosine, sine_rows = turn_table(positions)
+    queries = jnp.dot(normed, query_weight, preferred_element_type=jnp.float32).reshape(
+        row_count, head_count, NOPE + ROPE
+    )
+    query_plain = queries[..., :NOPE].astype(jnp.bfloat16)
+    query_turn = turn_rows(
+        queries[..., NOPE:], cosine.T[:, None, :], sine_rows.T[:, None, :]
+    ).astype(jnp.bfloat16)
+
+    kept = jnp.concatenate([near[:, width:], far[:, width:]], axis=0)
+    latents = kept[:, :latent_width]
+    turns = kept[:, latent_width : latent_width + ROPE]
+    places = []
+    for core in (0, 1):
+        for x_bit, y_bit in ((0, 0), (0, 2), (1, 0), (1, 2)):
+            for k in range(lines):
+                places.append(
+                    (ep_index ^ (2 * k + x_bit)) * row_count + (tp_index ^ (y_bit + core)) * piece
+                )
+    key_places = (jnp.stack(places)[:, None] + steps[None, :]).reshape(-1)
+    contract = (((0,), (1,)), ((), ()))
+    key_block = lax.dot_general(
+        key_weight, latents, contract, preferred_element_type=jnp.float32
+    ).astype(jnp.bfloat16)
+    value_block = lax.dot_general(
+        value_weight, latents, contract, preferred_element_type=jnp.float32
+    ).astype(jnp.bfloat16)
+    key_count = key_block.shape[1]
+    key_block = key_block.reshape(head_count, NOPE, key_count)
+    value_block = value_block.reshape(head_count, VD, key_count)
+    scores = jnp.einsum("ihd,hdj->hij", query_plain, key_block, preferred_element_type=jnp.float32)
+    scores = scores + jnp.einsum(
+        "ihd,jd->hij", query_turn, turns, preferred_element_type=jnp.float32
+    )
+    allowed = key_places[None, :] <= positions[:, None]
+    weights = jnp.where(allowed[None], jnp.exp(scores * (NOPE + ROPE) ** (-0.5)), 0.0)
+    weighted = jnp.einsum(
+        "hij,hdj->hid",
+        weights.astype(jnp.bfloat16),
+        value_block,
+        preferred_element_type=jnp.float32,
+    )
+    totals = jnp.sum(weights, axis=-1)
+    attended = (weighted / totals[..., None]).astype(jnp.bfloat16)
+    mixing = output_weight.reshape(head_count, VD, width)
+    partial_value = jnp.einsum("hid,hde->ie", attended, mixing, preferred_element_type=jnp.float32)
+    partial_value = partial_value.astype(jnp.bfloat16).reshape(2, 2, piece, width)
+    pair = add_pieces(partial_value[:, 0], swap(partial_value[:, 1], "tp", 1))
+    projected = pair[0].astype(jnp.float32) + swap(pair[1], "tp", 2).astype(jnp.float32)
+    mixed = rms_rows(projected, out_gain).astype(jnp.bfloat16)
+    return (mixed, moe_out)
+
+
+def local(*arrays):
+    routes = arrays[15]
+    tokens, choose = routes.shape
+    ep_size = lax.axis_size("ep")
+    tp_size = lax.axis_size("tp")
+    quarter_rows = tokens // tp_size
+    crowded = 2 * quarter_rows * choose // ep_size >= quarter_rows
+    paired = tp_size == 4 and ep_size >= 4 and ep_size & (ep_size - 1) == 0
+    if crowded and paired and ROPE + 2 * ep_size <= LANES:
+        return local_dense(*arrays)
+    return local_routed(*arrays)
+
 
 def solution(mesh):
     placed = (

time: 234 us -> 139 us (0.59)
  blocking collectives: 60.5 us -> 0 us
  waiting for transfers between devices: 81.7 us -> 57.4 us
  starting transfers between devices: 5.68 us -> 21.8 us
  matrix products: 30.5 us -> 14.4 us
  between operations: 14 us -> 0.92 us
  Pallas kernels: 0 us -> 10.8 us
  local copies, waits for them, and re-layouts: 26.4 us -> 17.1 us
    ppermute x0 -> x18, waiting for transfers between devices: none -> 57.4 us  [swap(): return lax.ppermute(array, axis, [(i, i ^ bit) for i in range(size)])]
    reduce_scatter x2 -> x0, waiting for transfers between devices: 45.1 us -> none  [local(): lax.psum_scatter(lax.optimization_barrier(partial_value.astype(jnp.bfloat...]
    all_to_all x1 -> x0, blocking collectives: 32.8 us -> none  [local(): lax.all_to_all(outgoing, 'ep', split_axis=1, concat_axis=1, tiled=True)]
    all_gather x2 -> x0, waiting for transfers between devices: 29.2 us -> none  [the longest x1 29.2 us: local(): row_block = lax.all_gather(arrived, 'tp', axis=0, tiled=True)]
    all_gather x1 -> x0, blocking collectives: 27.7 us -> none  [local(): lax.all_gather(rotary_key, 'ep', axis=1, tiled=True)]
    ppermute x0 -> x18, starting transfers between devices: none -> 21.8 us  [swap(): return lax.ppermute(array, axis, [(i, i ^ bit) for i in range(size)])]
    dot_general x11 -> x8, matrix products: 30.5 us -> 14.4 us  [the longest x1 3.84 us: local_dense(): jnp.einsum('hid,hde->ie', attended, mixing, preferred_element_type=jnp.fl...]
    pallas_call x0 -> x2, Pallas kernels: none -> 10.8 us  [apply_expert(): pl.pallas_call(lambda *refs: expert_rows(*refs, experts=experts), grid=(c...]
  transfers between devices with their start and end apart: 5 -> 18, of which waited for: 4 -> 10; matrix products, arithmetic and copies ran while one was open for 18% -> 18% of each run, Pallas kernels for 0% -> 4%
where the time goes in v1:
time: 139 us
  waiting for transfers between devices  57.4 us (41%)
  starting transfers between devices  21.8 us (16%)
  local copies, waits for them, and re-layouts  17.1 us (12%)
  other arithmetic  16.2 us (12%)
  matrix products  14.4 us (10%)
  Pallas kernels  10.8 us (8%)
    ppermute x18, waiting for transfers between devices, swap(): return lax.ppermute(array, axis, [(i, i ^ bit) for i in range(size)])  57.4 us
    ppermute x18, starting transfers between devices, swap(): return lax.ppermute(array, axis, [(i, i ^ bit) for i in range(size)])  21.8 us
    pallas_call x2, Pallas kernels, apply_expert(): pl.pallas_call(lambda *refs: expert_rows(*refs, experts=experts), grid=(c...  10.8 us
    unnamed x27, local copies, waits for them, and re-layouts  6.82 us
    convert_element_type x5, other arithmetic, add_pieces(): (left.astype(jnp.float32) + right.astype(jnp.float32)).astype(jnp.bfloat16)  4.53 us
    dot_general x1, matrix products, local_dense(): jnp.einsum('hid,hde->ie', attended, mixing, preferred_element_type=jnp.fl...  3.84 us
    slice x2, local copies, waits for them, and re-layouts, local_dense(): kept = jnp.concatenate([near[:, width:], far[:, width:]], axis=0)  3.11 us
    dot_general x1, matrix products, local_dense(): jnp.dot(own_normed, latent_weight, preferred_element_type=jnp.float32)  2.86 us
  transfers between devices with their start and end apart: 18, of which 10 were waited for; matrix products, arithmetic and copies ran while one was open for 18% of the time, Pallas kernels for 4%

profile of v1, /device:TPU:0, one launch (start us, length us, event | category | flops | bytes accessed | tf_op | source)
XLA Modules:
  0.0 138.6 jit_solution(17790023227550989810)
XLA Ops:
  5.7 1.7 %fusion.21 = (f32[32]{0:T(128)S(1)}, bf16[32,2048]{1,0:T(8,128)(2,1)S(1)}, f32[32]{0:T(128)}) fusion(bf16[128,2048]{1,0:T(8,128)(2,1)} %param.17, s32[]{:T(128)S(6)} %select_n.24, bf16[128,2048]{1,0:T(8,128)(2,1)} %param.27), kind=kLoop, calls=%fused_computation.40 | loop fusion | flops 393152 | bytes 393476 | tf_op jit(solution)/shard_map/reduce_sum | solution.py:20
  7.4 2.9 %multiply_reduce_fusion.1 = (f32[32]{0:T(128)S(1)}, f32[32,512]{1,0:T(8,128)}) fusion(bf16[2048,512]{1,0:T(8,128)(2,1)} %param.20, bf16[32,2048]{1,0:T(8,128)(2,1)S(1)} %get-tuple-element.3, f32[2048]{0:T(1024)} %param.18, f32[32]{0:T(128)S(1)} %add_rsqrt_fusion.2), kind=kOutput, calls=%fused_computation.75 | convolution fusion | flops 67403744 | bytes 2302208 | tf_op jit(solution)/shard_map/dot_general | solution.py:325
  11.8 1.7 %fusion.20 = bf16[32,2048]{1,0:T(8,128)(2,1)} fusion(f32[2048]{0:T(1024)} %param.28, f32[32]{0:T(128)S(1)} %add_rsqrt_fusion.3, bf16[128,2048]{1,0:T(8,128)(2,1)} %param.27, s32[]{:T(128)S(6)} %select_n.24), kind=kLoop, calls=%fused_computation.39 | loop fusion | flops 262144 | bytes 270468 | tf_op jit(solution)/shard_map/convert_element_type | solution.py:315
  16.2 3.1 %collective-permute-start = (bf16[1,32,2688]{2,1,0:T(8,128)(2,1)S(1)}, bf16[1,32,2688]{2,1,0:T(8,128)(2,1)S(1)}, u32[]{:S(2)}, u32[]{:S(2)}) collective-permute-start(bf16[1,32,2688]{2,1,0:T(8,128)(2,1)S(1)} %bitcast.128), channel_id=1, source_target_pairs={{0,8},{4,12},{8,0},{12,4},{16,24},{20,28},{24,16},{28,20},{1,9},{5... | collective-permute-start | bytes 516104 | tf_op jit(solution)/shard_map/ppermute | solution.py:309
  19.3 2.6 %collective-permute-start.1 = (bf16[1,32,2688]{2,1,0:T(8,128)(2,1)S(1)}, bf16[1,32,2688]{2,1,0:T(8,128)(2,1)S(1)}, u32[]{:S(2)}, u32[]{:S(2)}) collective-permute-start(bf16[1,32,2688]{2,1,0:T(8,128)(2,1)S(1)} %bitcast.129), channel_id=1, source_target_pairs={{0,16},{4,20},{8,24},{12,28},{16,0},{20,4},{24,8},{28,12},{1,17},{... | collective-permute-start | bytes 516104 | tf_op jit(solution)/shard_map/ppermute | solution.py:309
  22.6 3.8 %collective-permute-done = bf16[1,32,2688]{2,1,0:T(8,128)(2,1)S(1)} collective-permute-done((bf16[1,32,2688]{2,1,0:T(8,128)(2,1)S(1)}, bf16[1,32,2688]{2,1,0:T(8,128)(2,1)S(1)}, u32[]{:S(2)}, u32[]{:S(2)}) %collective-permute-start) | collective-permute-done | bytes 172064 | tf_op jit(solution)/shard_map/ppermute | solution.py:309
  26.4 8.4 %collective-permute-done.1 = bf16[1,32,2688]{2,1,0:T(8,128)(2,1)S(1)} collective-permute-done((bf16[1,32,2688]{2,1,0:T(8,128)(2,1)S(1)}, bf16[1,32,2688]{2,1,0:T(8,128)(2,1)S(1)}, u32[]{:S(2)}, u32[]{:S(2)}) %collective-permute-start.1) | collective-permute-done | bytes 172064 | tf_op jit(solution)/shard_map/ppermute | solution.py:309
  40.1 9.7 %collective-permute-done.3 = bf16[4,32,2688]{2,1,0:T(8,128)(2,1)S(1)} collective-permute-done((bf16[4,32,2688]{2,1,0:T(8,128)(2,1)S(1)}, bf16[4,32,2688]{2,1,0:T(8,128)(2,1)S(1)}, u32[]{:S(2)}, u32[]{:S(2)}) %collective-permute-start.3) | collective-permute-done | bytes 688160 | tf_op jit(solution)/shard_map/ppermute | solution.py:309
  55.2 3.2 %collective-permute-done.5 = bf16[2,32,2688]{2,1,0:T(8,128)(2,1)S(1)} collective-permute-done((bf16[2,32,2688]{2,1,0:T(8,128)(2,1)S(1)}, bf16[2,32,2688]{2,1,0:T(8,128)(2,1)S(1)}, u32[]{:S(2)}, u32[]{:S(2)}) %collective-permute-start.5) | collective-permute-done | bytes 344096 | tf_op jit(solution)/shard_map/ppermute | solution.py:309
  65.4 2.0 %slice.117 = bf16[512,640]{1,0:T(8,128)(2,1)} slice(bf16[512,2688]{1,0:T(8,128)(2,1)} %bitcast.34.refs_1_.refs_2_), slice={[0:512], [2048:2688]} | slice | bytes 1310720 | tf_op jit(solution)/shard_map/slice | solution.py:393
  67.3 5.4 %expert_rows.3 = bf16[512,2048]{1,0:T(8,128)(2,1)} custom-call(s32[1]{0:T(128)} %bitcast.48.refs_0_, bf16[512,2688]{1,0:T(8,128)(2,1)} %collective-permute-done.7.refs_1_.refs_2_, bf16[512,2688]{1,0:T(8,128)(2,1)} %collective-permute-done.7.refs_1_.refs_2_, bf16[2048,256]{1,0:T(8,128)(2,1)} %bitcast.122, bf16[2048,256]{1,0:T(8,128)(2,1)} %bitcast.124, ...), custom_call_target="tpu_custom_call" | custom-call | flops 1610612736 | bytes 7340032 | tf_op jit(solution)/shard_map/expert_rows/pallas_call | solution.py:251
  74.4 2.0 %convolution_convert_fusion.1 = bf16[1024,512]{0,1:T(8,128)(2,1)S(1)} fusion(bf16[512,512]{1,0:T(8,128)(2,1)} %param.23, bf16[512,640]{1,0:T(8,128)(2,1)} %slice.117, bf16[512,640]{1,0:T(8,128)(2,1)S(1)} %slice.118), kind=kOutput, calls=%fused_computation.8 | convolution fusion | flops 539492352 | bytes 2883584 | tf_op jit(solution)/shard_map/dot_general | solution.py:405
  77.6 1.7 %convolution_convert_fusion = bf16[1024,512]{0,1:T(8,128)(2,1)} fusion(bf16[512,512]{1,0:T(8,128)(2,1)S(1)} %copy-done.9, bf16[512,640]{1,0:T(8,128)(2,1)S(1)} %copy-done.1, bf16[512,640]{1,0:T(8,128)(2,1)S(1)} %slice.118), kind=kOutput, calls=%fused_computation.7 | convolution fusion | flops 539492352 | bytes 2883584 | tf_op jit(solution)/shard_map/dot_general | solution.py:408
  79.4 1.8 %fusion.56 = (f32[4,128]{1,0:T(4,128)S(1)}, bf16[4,128,1024]{2,1,0:T(8,128)(2,1)}) fusion(f32[4,128,1024]{2,1,0:T(8,128)S(1)} %fusion.30, bf16[128,4,32]{0,2,1:T(8,128)(2,1)S(1)} %get-tuple-element.12, bf16[128,4,32]{0,2,1:T(8,128)(2,1)S(1)} %get-tuple-element.11, bf16[512,640]{1,0:T(8,128)(2,1)S(1)} %slice.118, bf16[512,640]{1,0:T(8,128)(2,1)S(1)} %copy-done.1, ...), kind=kOutput, calls=%fused_computation.126 | convolution fusion | flops 70123008 | bytes 4655104 | tf_op jit(solution)/shard_map/ihd,jd->hij/dot_general | solution.py:415
  81.2 3.8 %fusion = bf16[128,2048]{1,0:T(8,128)(2,1)} fusion(bf16[4,128,2048]{2,1,0:T(8,128)(2,1)} %bitcast.137, bf16[4,128,1024]{2,1,0:T(8,128)(2,1)} %bitcast.138, bf16[4,128,1024]{2,1,0:T(8,128)(2,1)} %get-tuple-element.24, f32[4,128]{1,0:T(4,128)S(1)} %get-tuple-element.23), kind=kOutput, calls=%fused_computation.2 | convolution fusion | flops 403046400 | bytes 4720640 | tf_op jit(solution)/shard_map/hid,hde->ie/dot_general | solution.py:429
  85.0 1.7 %slice_bitcast_fusion.4 = bf16[2,32,2048]{2,1,0:T(8,128)(2,1)} fusion(bf16[2,2,32,2048]{3,2,1,0:T(8,128)(2,1)} %bitcast.133), kind=kLoop, calls=%fused_computation.47 | loop fusion | bytes 524288 | tf_op jit(solution)/shard_map/squeeze | solution.py:431
  86.7 5.4 %expert_rows.2 = bf16[512,2048]{1,0:T(8,128)(2,1)} custom-call(s32[1]{0:T(128)} %bitcast.48.refs_0_, bf16[512,2688]{1,0:T(8,128)(2,1)} %bitcast.34.refs_1_.refs_2_, bf16[512,2688]{1,0:T(8,128)(2,1)} %bitcast.34.refs_1_.refs_2_, bf16[2048,256]{1,0:T(8,128)(2,1)} %bitcast.123, bf16[2048,256]{1,0:T(8,128)(2,1)} %bitcast.125, bf16[256,2048]{1,0:T(8,128)(2,1)} %bitcast.127), custom_call_target="tpu_custom_call" | custom-call | flops 1610612736 | bytes 7340032 | tf_op jit(solution)/shard_map/expert_rows/pallas_call | solution.py:251
  93.2 3.0 %add_convert_fusion = bf16[512,2048]{1,0:T(8,128)(2,1)S(1)} fusion(bf16[512,2048]{1,0:T(8,128)(2,1)} %collective-permute-done.10, bf16[512,2048]{1,0:T(8,128)(2,1)} %expert_rows.2), kind=kLoop, calls=%fused_computation | loop fusion | flops 4194304 | bytes 6291456 | tf_op jit(solution)/shard_map/convert_element_type | solution.py:274
  97.9 2.1 %collective-permute-start.9 = (bf16[32,2048]{1,0:T(8,128)(2,1)S(1)}, bf16[32,2048]{1,0:T(8,128)(2,1)S(1)}, u32[]{:S(2)}, u32[]{:S(2)}) collective-permute-start(bf16[32,2048]{1,0:T(8,128)(2,1)S(1)} %slice_bitcast_fusion.10), channel_id=1, source_target_pairs={{0,2},{1,3},{2,0},{3,1},{4,6},{5,7},{6,4},{7,5},{8,10},{9,11},{10,... | collective-permute-start | bytes 393224 | tf_op jit(solution)/shard_map/ppermute | solution.py:309
  99.9 14.7 %collective-permute-done.9 = bf16[32,2048]{1,0:T(8,128)(2,1)S(1)} collective-permute-done((bf16[32,2048]{1,0:T(8,128)(2,1)S(1)}, bf16[32,2048]{1,0:T(8,128)(2,1)S(1)}, u32[]{:S(2)}, u32[]{:S(2)}) %collective-permute-start.9) | collective-permute-done | bytes 131104 | tf_op jit(solution)/shard_map/ppermute | solution.py:309
  116.3 6.6 %collective-permute-done.12 = bf16[2,32,2048]{2,1,0:T(8,128)(2,1)S(1)} collective-permute-done((bf16[2,32,2048]{2,1,0:T(8,128)(2,1)S(1)}, bf16[2,32,2048]{2,1,0:T(8,128)(2,1)S(1)}, u32[]{:S(2)}, u32[]{:S(2)}) %collective-permute-start.12) | collective-permute-done | bytes 262176 | tf_op jit(solution)/shard_map/ppermute | solution.py:309
  123.0 3.1 %collective-permute-start.13 = (bf16[32,2048]{1,0:T(8,128)(2,1)S(1)}, bf16[32,2048]{1,0:T(8,128)(2,1)S(1)}, u32[]{:S(2)}, u32[]{:S(2)}) collective-permute-start(bf16[32,2048]{1,0:T(8,128)(2,1)S(1)} %slice_bitcast_fusion.8), channel_id=1, source_target_pairs={{0,8},{4,12},{8,0},{12,4},{16,24},{20,28},{24,16},{28,20},{1,9},{5... | collective-permute-start | bytes 393224 | tf_op jit(solution)/shard_map/ppermute | solution.py:309
  126.2 1.7 %collective-permute-start.16 = (bf16[32,2048]{1,0:T(8,128)(2,1)S(1)}, bf16[32,2048]{1,0:T(8,128)(2,1)S(1)}, u32[]{:S(2)}, u32[]{:S(2)}) collective-permute-start(bf16[32,2048]{1,0:T(8,128)(2,1)S(1)} %get-tuple-element.13), channel_id=1, source_target_pairs={{0,16},{4,20},{8,24},{12,28},{16,0},{20,4},{24,8},{28,12},{1,17},{... | collective-permute-start | bytes 393224 | tf_op jit(solution)/shard_map/ppermute | solution.py:309
  130.3 7.6 %collective-permute-done.16 = bf16[32,2048]{1,0:T(8,128)(2,1)S(1)} collective-permute-done((bf16[32,2048]{1,0:T(8,128)(2,1)S(1)}, bf16[32,2048]{1,0:T(8,128)(2,1)S(1)}, u32[]{:S(2)}, u32[]{:S(2)}) %collective-permute-start.16) | collective-permute-done | bytes 131104 | tf_op jit(solution)/shard_map/ppermute | solution.py:309
  (103 shorter events, 37.9 us)
Async XLA Ops:
  0.6 62.5 %copy-start = (bf16[2048,768]{1,0:T(8,128)(2,1)S(1)}, bf16[2048,768]{1,0:T(8,128)(2,1)}, u32[]{:S(2)}) copy-start(bf16[2048,768]{1,0:T(8,128)(2,1)} %param.19) | copy-start | bytes 9437188
  0.6 10.2 %copy-start.4 = (bf16[2048,64]{0,1:T(8,128)(2,1)S(1)}, bf16[2048,64]{0,1:T(8,128)(2,1)}, u32[]{:S(2)}) copy-start(bf16[2048,64]{0,1:T(8,128)(2,1)} %param.21) | copy-start | bytes 786436
  5.7 5.1 %copy-start.5 = (f32[2048]{0:T(1024)S(1)}, f32[2048]{0:T(1024)}, u32[]{:S(2)}) copy-start(f32[2048]{0:T(1024)} %param.18) | copy-start | bytes 24580
  16.2 10.2 %collective-permute-start = (bf16[1,32,2688]{2,1,0:T(8,128)(2,1)S(1)}, bf16[1,32,2688]{2,1,0:T(8,128)(2,1)S(1)}, u32[]{:S(2)}, u32[]{:S(2)}) collective-permute-start(bf16[1,32,2688]{2,1,0:T(8,128)(2,1)S(1)} %bitcast.128), channel_id=1, source_target_pairs={{0,8},{4,12},{8,0},{12,4},{16,24},{20,28},{24,16},{28,20},{1,9},{5... | collective-permute-start | bytes 516104 | tf_op jit(solution)/shard_map/ppermute | solution.py:309
  19.3 15.5 %collective-permute-start.1 = (bf16[1,32,2688]{2,1,0:T(8,128)(2,1)S(1)}, bf16[1,32,2688]{2,1,0:T(8,128)(2,1)S(1)}, u32[]{:S(2)}, u32[]{:S(2)}) collective-permute-start(bf16[1,32,2688]{2,1,0:T(8,128)(2,1)S(1)} %bitcast.129), channel_id=1, source_target_pairs={{0,16},{4,20},{8,24},{12,28},{16,0},{20,4},{24,8},{28,12},{1,17},{... | collective-permute-start | bytes 516104 | tf_op jit(solution)/shard_map/ppermute | solution.py:309
  21.9 12.9 %collective-permute-start.2 = (bf16[1,32,2688]{2,1,0:T(8,128)(2,1)S(1)}, bf16[1,32,2688]{2,1,0:T(8,128)(2,1)S(1)}, u32[]{:S(2)}, u32[]{:S(2)}) collective-permute-start(bf16[1,32,2688]{2,1,0:T(8,128)(2,1)S(1)} %bitcast.130), channel_id=1, source_target_pairs={{0,24},{4,28},{8,16},{12,20},{16,8},{20,12},{24,0},{28,4},{1,25},{... | collective-permute-start | bytes 516104 | tf_op jit(solution)/shard_map/ppermute | solution.py:309
  35.0 14.8 %collective-permute-start.3 = (bf16[4,32,2688]{2,1,0:T(8,128)(2,1)S(1)}, bf16[4,32,2688]{2,1,0:T(8,128)(2,1)S(1)}, u32[]{:S(2)}, u32[]{:S(2)}) collective-permute-start(bf16[4,32,2688]{2,1,0:T(8,128)(2,1)S(1)} %pad_maximum_fusion), channel_id=1, source_target_pairs={{0,2},{1,3},{2,0},{3,1},{4,6},{5,7},{6,4},{7,5},{8,10},{9,11},{10,... | collective-permute-start | bytes 2064392 | tf_op jit(solution)/shard_map/ppermute | solution.py:309
  36.5 16.5 %collective-permute-start.4 = (bf16[4,32,2688]{2,1,0:T(8,128)(2,1)S(1)}, bf16[4,32,2688]{2,1,0:T(8,128)(2,1)S(1)}, u32[]{:S(2)}, u32[]{:S(2)}) collective-permute-start(bf16[4,32,2688]{2,1,0:T(8,128)(2,1)S(1)} %pad_maximum_fusion), channel_id=1, source_target_pairs={{0,4},{4,0},{8,12},{12,8},{16,20},{20,16},{24,28},{28,24},{1,5},{5... | collective-permute-start | bytes 2064392 | tf_op jit(solution)/shard_map/ppermute | solution.py:309
  49.8 8.6 %collective-permute-start.5 = (bf16[2,32,2688]{2,1,0:T(8,128)(2,1)S(1)}, bf16[2,32,2688]{2,1,0:T(8,128)(2,1)S(1)}, u32[]{:S(2)}, u32[]{:S(2)}) collective-permute-start(bf16[2,32,2688]{2,1,0:T(8,128)(2,1)S(1)} %slice.115), channel_id=1, source_target_pairs={{0,4},{4,0},{8,12},{12,8},{16,20},{20,16},{24,28},{28,24},{1,5},{5... | collective-permute-start | bytes 1032200 | tf_op jit(solution)/shard_map/ppermute | solution.py:309
  53.1 7.3 %collective-permute-start.6 = (bf16[2,32,2688]{2,1,0:T(8,128)(2,1)S(1)}, bf16[2,32,2688]{2,1,0:T(8,128)(2,1)S(1)}, u32[]{:S(2)}, u32[]{:S(2)}) collective-permute-start(bf16[2,32,2688]{2,1,0:T(8,128)(2,1)S(1)} %slice.116), channel_id=1, source_target_pairs={{0,2},{1,3},{2,0},{3,1},{4,6},{5,7},{6,4},{7,5},{8,10},{9,11},{10,... | collective-permute-start | bytes 1032200 | tf_op jit(solution)/shard_map/ppermute | solution.py:309
  54.3 8.6 %copy-start.8 = (f32[32]{0:T(128)S(1)}, f32[32]{0:T(128)}, u32[]{:S(2)}) copy-start(f32[32]{0:T(128)} %multiply_power_fusion) | copy-start | bytes 388
  54.3 8.9 %copy-start.6 = (f32[2048]{0:T(1024)S(1)}, f32[2048]{0:T(1024)}, u32[]{:S(2)}) copy-start(f32[2048]{0:T(1024)} %param.18) | copy-start | bytes 24580
  61.1 6.2 %collective-permute-start.7 = (bf16[512,2688]{1,0:T(8,128)(2,1)}, bf16[512,2688]{1,0:T(8,128)(2,1)}, u32[]{:S(2)}, u32[]{:S(2)}) collective-permute-start(bf16[512,2688]{1,0:T(8,128)(2,1)} %bitcast.34.refs_1_.refs_2_), channel_id=1, source_target_pairs={{0,1},{1,0},{2,3},{3,2},{4,5},{5,4},{6,7},{7,6},{8,9},{9,8},{10,11... | collective-permute-start | bytes 8257544 | tf_op jit(solution)/shard_map/ppermute | solution.py:309
  72.7 20.4 %collective-permute-start.10 = (bf16[512,2048]{1,0:T(8,128)(2,1)}, bf16[512,2048]{1,0:T(8,128)(2,1)}, u32[]{:S(2)}, u32[]{:S(2)}) collective-permute-start(bf16[512,2048]{1,0:T(8,128)(2,1)} %expert_rows.3), channel_id=1, source_target_pairs={{0,1},{1,0},{2,3},{3,2},{4,5},{5,4},{6,7},{7,6},{8,9},{9,8},{10,11... | collective-permute-start | bytes 6291464 | tf_op jit(solution)/shard_map/ppermute | solution.py:309
  86.7 5.4 %collective-permute-start.8 = (bf16[2,32,2048]{2,1,0:T(8,128)(2,1)}, bf16[2,32,2048]{2,1,0:T(8,128)(2,1)S(1)}, u32[]{:S(2)}, u32[]{:S(2)}) collective-permute-start(bf16[2,32,2048]{2,1,0:T(8,128)(2,1)} %slice_bitcast_fusion.4), channel_id=1, source_target_pairs={{0,1},{1,0},{2,3},{3,2},{4,5},{5,4},{6,7},{7,6},{8,9},{9,8},{10,11... | collective-permute-start | bytes 786440 | tf_op jit(solution)/shard_map/ppermute | solution.py:309
  96.3 18.6 %collective-permute-start.11 = (bf16[2,2,32,2048]{3,2,1,0:T(8,128)(2,1)S(1)}, bf16[2,2,32,2048]{3,2,1,0:T(8,128)(2,1)S(1)}, u32[]{:S(2)}, u32[]{:S(2)}) collective-permute-start(bf16[2,2,32,2048]{3,2,1,0:T(8,128)(2,1)S(1)} %get-tuple-element.6), channel_id=1, source_target_pairs={{0,4},{4,0},{8,12},{12,8},{16,20},{20,16},{24,28},{28,24},{1,5},{5... | collective-permute-start | bytes 1572872 | tf_op jit(solution)/shard_map/ppermute | solution.py:309
  97.8 17.0 %collective-permute-start.14 = (bf16[2,2,32,2048]{3,2,1,0:T(8,128)(2,1)S(1)}, bf16[2,2,32,2048]{3,2,1,0:T(8,128)(2,1)S(1)}, u32[]{:S(2)}, u32[]{:S(2)}) collective-permute-start(bf16[2,2,32,2048]{3,2,1,0:T(8,128)(2,1)S(1)} %get-tuple-element.7), channel_id=1, source_target_pairs={{0,2},{1,3},{2,0},{3,1},{4,6},{5,7},{6,4},{7,5},{8,10},{9,11},{10,... | collective-permute-start | bytes 1572872 | tf_op jit(solution)/shard_map/ppermute | solution.py:309
  97.9 16.8 %collective-permute-start.9 = (bf16[32,2048]{1,0:T(8,128)(2,1)S(1)}, bf16[32,2048]{1,0:T(8,128)(2,1)S(1)}, u32[]{:S(2)}, u32[]{:S(2)}) collective-permute-start(bf16[32,2048]{1,0:T(8,128)(2,1)S(1)} %slice_bitcast_fusion.10), channel_id=1, source_target_pairs={{0,2},{1,3},{2,0},{3,1},{4,6},{5,7},{6,4},{7,5},{8,10},{9,11},{10,... | collective-permute-start | bytes 393224 | tf_op jit(solution)/shard_map/ppermute | solution.py:309
  115.3 13.9 %copy-start.7 = (f32[2048]{0:T(1024)S(1)}, f32[2048]{0:T(1024)}, u32[]{:S(2)}) copy-start(f32[2048]{0:T(1024)} %param.26) | copy-start | bytes 24580
  115.3 7.6 %collective-permute-start.12 = (bf16[2,32,2048]{2,1,0:T(8,128)(2,1)S(1)}, bf16[2,32,2048]{2,1,0:T(8,128)(2,1)S(1)}, u32[]{:S(2)}, u32[]{:S(2)}) collective-permute-start(bf16[2,32,2048]{2,1,0:T(8,128)(2,1)S(1)} %slice_bitcast_fusion.2), channel_id=1, source_target_pairs={{0,2},{1,3},{2,0},{3,1},{4,6},{5,7},{6,4},{7,5},{8,10},{9,11},{10,... | collective-permute-start | bytes 786440 | tf_op jit(solution)/shard_map/ppermute | solution.py:309
  115.7 10.4 %collective-permute-start.15 = (bf16[2,32,2048]{2,1,0:T(8,128)(2,1)S(1)}, bf16[2,32,2048]{2,1,0:T(8,128)(2,1)S(1)}, u32[]{:S(2)}, u32[]{:S(2)}) collective-permute-start(bf16[2,32,2048]{2,1,0:T(8,128)(2,1)S(1)} %slice_bitcast_fusion), channel_id=1, source_target_pairs={{0,4},{4,0},{8,12},{12,8},{16,20},{20,16},{24,28},{28,24},{1,5},{5... | collective-permute-start | bytes 786440 | tf_op jit(solution)/shard_map/ppermute | solution.py:309
  123.0 7.2 %collective-permute-start.13 = (bf16[32,2048]{1,0:T(8,128)(2,1)S(1)}, bf16[32,2048]{1,0:T(8,128)(2,1)S(1)}, u32[]{:S(2)}, u32[]{:S(2)}) collective-permute-start(bf16[32,2048]{1,0:T(8,128)(2,1)S(1)} %slice_bitcast_fusion.8), channel_id=1, source_target_pairs={{0,8},{4,12},{8,0},{12,4},{16,24},{20,28},{24,16},{28,20},{1,9},{5... | collective-permute-start | bytes 393224 | tf_op jit(solution)/shard_map/ppermute | solution.py:309
  126.2 11.7 %collective-permute-start.16 = (bf16[32,2048]{1,0:T(8,128)(2,1)S(1)}, bf16[32,2048]{1,0:T(8,128)(2,1)S(1)}, u32[]{:S(2)}, u32[]{:S(2)}) collective-permute-start(bf16[32,2048]{1,0:T(8,128)(2,1)S(1)} %get-tuple-element.13), channel_id=1, source_target_pairs={{0,16},{4,20},{8,24},{12,28},{16,0},{20,4},{24,8},{28,12},{1,17},{... | collective-permute-start | bytes 393224 | tf_op jit(solution)/shard_map/ppermute | solution.py:309
  127.9 9.9 %collective-permute-start.17 = (bf16[32,2048]{1,0:T(8,128)(2,1)S(1)}, bf16[32,2048]{1,0:T(8,128)(2,1)S(1)}, u32[]{:S(2)}, u32[]{:S(2)}) collective-permute-start(bf16[32,2048]{1,0:T(8,128)(2,1)S(1)} %get-tuple-element.14), channel_id=1, source_target_pairs={{0,24},{4,28},{8,16},{12,20},{16,8},{20,12},{24,0},{28,4},{1,25},{... | collective-permute-start | bytes 393224 | tf_op jit(solution)/shard_map/ppermute | solution.py:309
  (4 other events, 5.1 us)

commit v2 on v1

--- a/solution.py
+++ b/solution.py
@@ -270,6 +270,119 @@
     )(expert, block, block, gate_w, up_w, down_w)
 
 
+def own_rows(
+    place_ref,
+    ffn_ref,
+    ffn_gain_ref,
+    mix_ref,
+    mix_gain_ref,
+    latent_weight_ref,
+    latent_gain_ref,
+    rotary_ref,
+    inverse_ref,
+    routes_ref,
+    scores_ref,
+    out_ref,
+    shares_ref,
+    *,
+    piece,
+    experts,
+):
+    width = ffn_ref.shape[1]
+    latent_width = latent_weight_ref.shape[1]
+    out_ref[:, :width] = rms_rows(ffn_ref[...].astype(jnp.float32), ffn_gain_ref[...]).astype(
+        jnp.bfloat16
+    )
+    normed = rms_rows(mix_ref[...].astype(jnp.float32), mix_gain_ref[...]).astype(jnp.bfloat16)
+    latent = jnp.dot(normed, latent_weight_ref[...], preferred_element_type=jnp.float32)
+    out_ref[:, width : width + latent_width] = rms_rows(latent, latent_gain_ref[...]).astype(
+        jnp.bfloat16
+    )
+    rotary = lax.dot_general(
+        normed, rotary_ref[...], (((1,), (1,)), ((), ())), preferred_element_type=jnp.float32
+    )
+    half_rope = ROPE // 2
+    swapped = jnp.concatenate([rotary[:, half_rope:], rotary[:, :half_rope]], axis=1)
+    first = place_ref[1]
+    rows = lax.broadcasted_iota(jnp.int32, rotary.shape, 0) + first
+    angles = rows.astype(jnp.float32) * inverse_ref[...]
+    upper = lax.broadcasted_iota(jnp.int32, rotary.shape, 1) < half_rope
+    sines = jnp.sin(angles)
+    turned = rotary * jnp.cos(angles) + swapped * jnp.where(upper, -sines, sines)
+    scores = scores_ref[...]
+    powers = jnp.exp(scores - jnp.max(scores, axis=0, keepdims=True))
+    gate_share = powers / jnp.sum(powers, axis=0, keepdims=True)
+    named = routes_ref[...]
+    choose, tokens = scores.shape
+    ids = lax.broadcasted_iota(jnp.int32, (experts, tokens), 0)
+    shares = jnp.zeros((experts, tokens), jnp.float32)
+    for k in range(choose):
+        shares = shares + jnp.where(named[k : k + 1] == ids, gate_share[k : k + 1], 0.0)
+    high = shares.astype(jnp.bfloat16).astype(jnp.float32)
+    side_width = out_ref.shape[1] - width - latent_width
+    table = jnp.concatenate(
+        [
+            jnp.zeros((ROPE, tokens), jnp.float32),
+            high,
+            shares - high,
+            jnp.zeros((side_width - ROPE - 2 * experts, tokens), jnp.float32),
+        ],
+        axis=0,
+    )
+    shares_ref[...] = table.T
+    own_shares = shares_ref[pl.ds(pl.multiple_of(place_ref[0] * piece, piece), piece), :]
+    turned = jnp.concatenate(
+        [turned, jnp.zeros((piece, side_width - ROPE), jnp.float32)], axis=1
+    )
+    out_ref[:, width + latent_width :] = (own_shares + turned).astype(jnp.bfloat16)
+
+
+def own_piece(
+    place,
+    ffn_in,
+    ffn_gain,
+    mix_in,
+    mix_gain,
+    latent_weight,
+    latent_gain,
+    rotary_weight,
+    routes,
+    route_scores,
+    piece,
+    experts,
+):
+    tokens, width = ffn_in.shape
+    latent_width = latent_weight.shape[1]
+    side_width = LANES
+    inverse = rope_base ** (-jnp.arange(0, ROPE, 2).astype(jnp.float32) / ROPE)
+    inverse = jnp.concatenate([inverse, inverse])[None]
+    own_block = pl.BlockSpec((piece, width), lambda i, place: (place[0], 0))
+    whole = lambda array: pl.BlockSpec(array.shape, lambda i, place: (0, 0))
+    others = [
+        mix_gain[None],
+        latent_weight,
+        latent_gain[None],
+        rotary_weight.T,
+        inverse,
+        routes.T,
+        route_scores.T,
+    ]
+    ffn_gain = ffn_gain[None]
+    total = width + latent_width + side_width
+    return pl.pallas_call(
+        lambda *refs: own_rows(*refs, piece=piece, experts=experts),
+        grid_spec=pltpu.PrefetchScalarGridSpec(
+            num_scalar_prefetch=1,
+            grid=(1,),
+            in_specs=[own_block, whole(ffn_gain), own_block] + [whole(array) for array in others],
+            out_specs=pl.BlockSpec((piece, total), lambda i, place: (0, 0)),
+            scratch_shapes=[pltpu.VMEM((tokens, side_width), jnp.float32)],
+        ),
+        out_shape=jax.ShapeDtypeStruct((piece, total), jnp.bfloat16),
+        name="own_rows",
+    )(place, ffn_in, ffn_gain, mix_in, *others)
+
+
 def add_pieces(left, right):
     return (left.astype(jnp.float32) + right.astype(jnp.float32)).astype(jnp.bfloat16)
 
@@ -308,40 +421,44 @@
         size = ep_size if axis == "ep" else tp_size
         return lax.ppermute(array, axis, [(i, i ^ bit) for i in range(size)])
 
-    own_rows = lax.dynamic_slice_in_dim(ffn_in, tp_index * piece, piece, 0)
-    own_routes = lax.dynamic_slice_in_dim(routes, tp_index * piece, piece, 0)
-    own_scores = lax.dynamic_slice_in_dim(route_scores, tp_index * piece, piece, 0)
-    own_mix = lax.dynamic_slice_in_dim(mix_in, tp_index * piece, piece, 0)
-    normed_b = rms_rows(own_rows.astype(jnp.float32), ffn_gain).astype(jnp.bfloat16)
-    gate_share = jax.nn.softmax(own_scores, axis=-1)
-    named = own_routes[:, :, None] == jnp.arange(experts, dtype=jnp.int32)[None, None, :]
-    shares = jnp.sum(jnp.where(named, gate_share[:, :, None], 0.0), axis=1)
-    shares_high = lax.reduce_precision(shares, 8, 7)
-    shares_low = shares - shares_high
-    own_first = ep_index * row_count + tp_index * piece
-    own_cos, own_sin = turn_table(own_first + jnp.arange(piece, dtype=jnp.int32))
-    own_normed = rms_rows(own_mix.astype(jnp.float32), mix_gain).astype(jnp.bfloat16)
-    latent = rms_rows(
-        jnp.dot(own_normed, latent_weight, preferred_element_type=jnp.float32), latent_gain
+    place = jnp.stack([tp_index, ep_index * row_count + tp_index * piece]).astype(jnp.int32)
+    own = own_piece(
+        place,
+        ffn_in,
+        ffn_gain,
+        mix_in,
+        mix_gain,
+        latent_weight,
+        latent_gain,
+        rotary_weight,
+        routes,
+        route_scores,
+        piece,
+        experts,
+    )[None]
+
+    order = tp_index ^ jnp.arange(tp_size, dtype=jnp.int32)
+    mix_rows = jnp.concatenate(
+        [
+            lax.dynamic_slice_in_dim(mix_in, (tp_index ^ k) * piece, piece, 0)
+            for k in range(tp_size)
+        ],
+        axis=0,
+    )
+    steps = jnp.arange(piece, dtype=jnp.int32)
+    positions = (ep_index * row_count + order[:, None] * piece + steps[None, :]).reshape(-1)
+    normed = rms_rows(mix_rows.astype(jnp.float32), mix_gain).astype(jnp.bfloat16)
+    cosine, sine_rows = turn_table(positions)
+    queries = jnp.dot(normed, query_weight, preferred_element_type=jnp.float32).reshape(
+        row_count, head_count, NOPE + ROPE
+    )
+    query_plain = queries[..., :NOPE].astype(jnp.bfloat16)
+    query_turn = turn_rows(
+        queries[..., NOPE:], cosine.T[:, None, :], sine_rows.T[:, None, :]
     ).astype(jnp.bfloat16)
-    rotary_key = turn_rows(
-        jnp.dot(own_normed, rotary_weight, preferred_element_type=jnp.float32),
-        own_cos.T,
-        own_sin.T,
-    ).astype(jnp.bfloat16)
-    used = ROPE + 2 * experts
-    side = jnp.concatenate(
-        [
-            rotary_key,
-            shares_high.astype(jnp.bfloat16),
-            shares_low.astype(jnp.bfloat16),
-            jnp.zeros((piece, -used % LANES), jnp.bfloat16),
-        ],
-        axis=1,
-    )
-    own = jnp.concatenate([normed_b, latent, side], axis=1)[None]
 
     line = jnp.concatenate([own] + [swap(own, "ep", 2 * k) for k in range(1, lines)], axis=0)
+    line, query_plain, query_turn = lax.optimization_barrier((line, query_plain, query_turn))
     from_x = swap(line, "ep", 1)
     from_y = swap(line, "tp", 2)
     half = lines // 2
@@ -353,44 +470,14 @@
     expert = ep_index.astype(jnp.int32).reshape(1)
     weights_of = (gate_weight[0], up_weight[0], down_weight[0])
     near_out = apply_expert(expert, near, *weights_of, latent_width, experts)
+    near_out, far = lax.optimization_barrier((near_out, far))
     far_out = apply_expert(expert, far, *weights_of, latent_width, experts)
 
-    blocks = add_pieces(near_out, swap(far_out, "tp", 1)).reshape(4, lines, piece, width)
-    got_x = swap(blocks[2:, :half], "ep", 1)
-    got_y = swap(blocks[1::2, half:], "tp", 2)
-    first = add_pieces(blocks[:2, :half], got_x)
-    second = add_pieces(blocks[0::2, half:], got_y)
-    got_y = swap(first[1], "tp", 2)
-    got_x = swap(second[1], "ep", 1)
-    summed = jnp.concatenate(
-        [add_pieces(first[0], got_y), add_pieces(second[0], got_x)], axis=0
-    )
-    moe_sum = summed[0].astype(jnp.float32)
-    for k in range(1, lines):
-        moe_sum = moe_sum + swap(summed[k], "ep", 2 * k).astype(jnp.float32)
-    moe_out = moe_sum.astype(jnp.bfloat16)
-
-    order = tp_index ^ jnp.arange(tp_size, dtype=jnp.int32)
-    mix_rows = jnp.concatenate(
-        [
-            lax.dynamic_slice_in_dim(mix_in, (tp_index ^ k) * piece, piece, 0)
-            for k in range(tp_size)
-        ],
-        axis=0,
-    )
-    steps = jnp.arange(piece, dtype=jnp.int32)
-    positions = (ep_index * row_count + order[:, None] * piece + steps[None, :]).reshape(-1)
-    normed = rms_rows(mix_rows.astype(jnp.float32), mix_gain).astype(jnp.bfloat16)
-    cosine, sine_rows = turn_table(positions)
-    queries = jnp.dot(normed, query_weight, preferred_element_type=jnp.float32).reshape(
-        row_count, head_count, NOPE + ROPE
-    )
-    query_plain = queries[..., :NOPE].astype(jnp.bfloat16)
-    query_turn = turn_rows(
-        queries[..., NOPE:], cosine.T[:, None, :], sine_rows.T[:, None, :]
-    ).astype(jnp.bfloat16)
-
-    kept = jnp.concatenate([near[:, width:], far[:, width:]], axis=0)
+    far_out, near_kept, far_kept = lax.optimization_barrier(
+        (far_out, near[:, width:], far[:, width:])
+    )
+
+    kept = jnp.concatenate([near_kept, far_kept], axis=0)
     latents = kept[:, :latent_width]
     turns = kept[:, latent_width : latent_width + ROPE]
     places = []
@@ -411,6 +498,24 @@
     key_count = key_block.shape[1]
     key_block = key_block.reshape(head_count, NOPE, key_count)
     value_block = value_block.reshape(head_count, VD, key_count)
+    blocks = add_pieces(near_out, swap(far_out, "tp", 1)).reshape(4, lines, piece, width)
+    sent_x, sent_y, key_block, value_block, turns = lax.optimization_barrier(
+        (blocks[2:, :half], blocks[1::2, half:], key_block, value_block, turns)
+    )
+    got_x = swap(sent_x, "ep", 1)
+    got_y = swap(sent_y, "tp", 2)
+    first = add_pieces(blocks[:2, :half], got_x)
+    second = add_pieces(blocks[0::2, half:], got_y)
+    got_y = swap(first[1], "tp", 2)
+    got_x = swap(second[1], "ep", 1)
+    summed = jnp.concatenate(
+        [add_pieces(first[0], got_y), add_pieces(second[0], got_x)], axis=0
+    )
+    moe_sum = summed[0].astype(jnp.float32)
+    for k in range(1, lines):
+        moe_sum = moe_sum + swap(summed[k], "ep", 2 * k).astype(jnp.float32)
+    moe_out = moe_sum.astype(jnp.bfloat16)
+
     scores = jnp.einsum("ihd,hdj->hij", query_plain, key_block, preferred_element_type=jnp.float32)
     scores = scores + jnp.einsum(
         "ihd,jd->hij", query_turn, turns, preferred_element_type=jnp.float32

time: 139 us -> 128 us (0.921)
  other arithmetic: 16.2 us -> 9.75 us
  matrix products: 14.4 us -> 10.1 us
  Pallas kernels: 10.8 us -> 14.7 us
  waiting for transfers between devices: 57.4 us -> 54.9 us
  local copies, waits for them, and re-layouts: 17.1 us -> 15.3 us
    pallas_call x0 -> x1, Pallas kernels: none -> 3.97 us  [own_piece(): pl.pallas_call(lambda *refs: own_rows(*refs, piece=piece, experts=experts...]
    dot_general x2 -> x0, matrix products: 3.11 us -> none  [the longest x1 2.86 us: local_dense(): jnp.dot(own_normed, latent_weight, preferred_element_type=jnp.float32)]
    convert_element_type x3 -> x0, other arithmetic: 2.62 us -> none  [the longest x1 1.68 us: local_dense(): rms_rows(own_rows.astype(jnp.float32), ffn_gain).astype(jnp.bfloat16)]
    ppermute x18, waiting for transfers between devices: 57.4 us -> 54.9 us  [swap(): return lax.ppermute(array, axis, [(i, i ^ bit) for i in range(size)])]
    slice x3 -> x5, local copies, waits for them, and re-layouts: 3.21 us -> 5.22 us  [the longest x1 2.06 us: local_dense(): near[:, width:]]
    reduce_sum x3 -> x2, other arithmetic: 2 us -> 0.34 us  [rms_rows(): mean_square = jnp.mean(rows_in * rows_in, axis=-1, keepdims=True)]
    unnamed x27 -> x21, local copies, waits for them, and re-layouts: 6.82 us -> 5.58 us
  transfers between devices with their start and end apart: 18 -> 18, of which waited for: 10 -> 8; matrix products, arithmetic and copies ran while one was open for 18% -> 13% of each run, Pallas kernels for 4% -> 4%
where the time goes in v2:
time: 128 us; the launch traced here: 127 us
  waiting for transfers between devices  54.9 us (43%)
  starting transfers between devices  21.5 us (17%)
  local copies, waits for them, and re-layouts  15.3 us (12%)
  Pallas kernels  14.7 us (11%)
  matrix products  10.1 us (8%)
  other arithmetic  9.75 us (8%)
    ppermute x18, waiting for transfers between devices, swap(): return lax.ppermute(array, axis, [(i, i ^ bit) for i in range(size)])  54.9 us
    ppermute x18, starting transfers between devices, swap(): return lax.ppermute(array, axis, [(i, i ^ bit) for i in range(size)])  21.5 us
    pallas_call x2, Pallas kernels, apply_expert(): pl.pallas_call(lambda *refs: expert_rows(*refs, experts=experts), grid=(c...  10.8 us
    unnamed x21, local copies, waits for them, and re-layouts  5.58 us
    convert_element_type x5, other arithmetic, add_pieces(): (left.astype(jnp.float32) + right.astype(jnp.float32)).astype(jnp.bfloat16)  5.1 us
    pallas_call x1, Pallas kernels, own_piece(): pl.pallas_call(lambda *refs: own_rows(*refs, piece=piece, experts=experts...  3.97 us
    dot_general x1, matrix products, local_dense(): jnp.einsum('hid,hde->ie', attended, mixing, preferred_element_type=jnp.fl...  3.83 us
  transfers between devices with their start and end apart: 18, of which 8 were waited for; matrix products, arithmetic and copies ran while one was open for 13% of the time, Pallas kernels for 4%

profile of v2, /device:TPU:0, one launch (start us, length us, event | category | flops | bytes accessed | tf_op | source)
XLA Modules:
  0.0 127.2 jit_solution(1540625219840419336)
XLA Ops:
  1.9 4.0 %own_rows.1 = bf16[32,2688]{1,0:T(8,128)(2,1)} custom-call(s32[2]{0:T(128)} %pad_add_fusion.refs_0_, bf16[128,2048]{1,0:T(8,128)(2,1)} %refs_1_.1, f32[1,2048]{1,0:T(1,128)} %bitcast.146, bf16[128,2048]{1,0:T(8,128)(2,1)} %refs_3_.1, f32[1,2048]{1,0:T(1,128)} %bitcast.147, bf16[2048,512]{1,0:T(8,128)(2,1)} %refs_5_.1, f32[1,512]{1,0:T(1,128)} %bitcast.148, ...), custom_call_target="tpu_custom_call" | custom-call | tf_op jit(solution)/shard_map/own_rows/pallas_call | solution.py:372
  5.9 5.1 %collective-permute-start.2 = (bf16[1,32,2688]{2,1,0:T(8,128)(2,1)}, bf16[1,32,2688]{2,1,0:T(8,128)(2,1)S(1)}, u32[]{:S(2)}, u32[]{:S(2)}) collective-permute-start(bf16[1,32,2688]{2,1,0:T(8,128)(2,1)} %bitcast.137), channel_id=1, source_target_pairs={{0,24},{4,28},{8,16},{12,20},{16,8},{20,12},{24,0},{28,4},{1,25},{... | collective-permute-start | bytes 516104 | tf_op jit(solution)/shard_map/ppermute | solution.py:422
  14.7 1.8 %collective-permute-done.2 = bf16[1,32,2688]{2,1,0:T(8,128)(2,1)S(1)} collective-permute-done((bf16[1,32,2688]{2,1,0:T(8,128)(2,1)}, bf16[1,32,2688]{2,1,0:T(8,128)(2,1)S(1)}, u32[]{:S(2)}, u32[]{:S(2)}) %collective-permute-start.2) | collective-permute-done | bytes 172064 | tf_op jit(solution)/shard_map/ppermute | solution.py:422
  16.5 9.4 %collective-permute-done.1 = bf16[1,32,2688]{2,1,0:T(8,128)(2,1)} collective-permute-done((bf16[1,32,2688]{2,1,0:T(8,128)(2,1)}, bf16[1,32,2688]{2,1,0:T(8,128)(2,1)}, u32[]{:S(2)}, u32[]{:S(2)}) %collective-permute-start.1) | collective-permute-done | bytes 172064 | tf_op jit(solution)/shard_map/ppermute | solution.py:422
  27.0 1.6 %collective-permute-start.4 = (bf16[4,32,2688]{2,1,0:T(8,128)(2,1)S(1)}, bf16[4,32,2688]{2,1,0:T(8,128)(2,1)S(1)}, u32[]{:S(2)}, u32[]{:S(2)}) collective-permute-start(bf16[4,32,2688]{2,1,0:T(8,128)(2,1)S(1)} %pad_maximum_fusion), channel_id=1, source_target_pairs={{0,4},{4,0},{8,12},{12,8},{16,20},{20,16},{24,28},{28,24},{1,5},{5... | collective-permute-start | bytes 2064392 | tf_op jit(solution)/shard_map/ppermute | solution.py:422
  30.9 12.6 %collective-permute-done.4 = bf16[4,32,2688]{2,1,0:T(8,128)(2,1)S(1)} collective-permute-done((bf16[4,32,2688]{2,1,0:T(8,128)(2,1)S(1)}, bf16[4,32,2688]{2,1,0:T(8,128)(2,1)S(1)}, u32[]{:S(2)}, u32[]{:S(2)}) %collective-permute-start.4) | collective-permute-done | bytes 688160 | tf_op jit(solution)/shard_map/ppermute | solution.py:422
  43.6 1.6 %collective-permute-start.6 = (bf16[2,32,2688]{2,1,0:T(8,128)(2,1)S(1)}, bf16[2,32,2688]{2,1,0:T(8,128)(2,1)S(1)}, u32[]{:S(2)}, u32[]{:S(2)}) collective-permute-start(bf16[2,32,2688]{2,1,0:T(8,128)(2,1)S(1)} %slice.108), channel_id=1, source_target_pairs={{0,2},{1,3},{2,0},{3,1},{4,6},{5,7},{6,4},{7,5},{8,10},{9,11},{10,... | collective-permute-start | bytes 1032200 | tf_op jit(solution)/shard_map/ppermute | solution.py:422
  45.2 1.6 %collective-permute-start.5 = (bf16[2,32,2688]{2,1,0:T(8,128)(2,1)S(1)}, bf16[2,32,2688]{2,1,0:T(8,128)(2,1)S(1)}, u32[]{:S(2)}, u32[]{:S(2)}) collective-permute-start(bf16[2,32,2688]{2,1,0:T(8,128)(2,1)S(1)} %slice.107), channel_id=1, source_target_pairs={{0,4},{4,0},{8,12},{12,8},{16,20},{20,16},{24,28},{28,24},{1,5},{5... | collective-permute-start | bytes 1032200 | tf_op jit(solution)/shard_map/ppermute | solution.py:422
  48.6 4.7 %collective-permute-done.5 = bf16[2,32,2688]{2,1,0:T(8,128)(2,1)S(1)} collective-permute-done((bf16[2,32,2688]{2,1,0:T(8,128)(2,1)S(1)}, bf16[2,32,2688]{2,1,0:T(8,128)(2,1)S(1)}, u32[]{:S(2)}, u32[]{:S(2)}) %collective-permute-start.5) | collective-permute-done | bytes 344096 | tf_op jit(solution)/shard_map/ppermute | solution.py:422
  54.8 2.1 %slice.109 = bf16[512,640]{1,0:T(8,128)(2,1)} slice(bf16[512,2688]{1,0:T(8,128)(2,1)} %bitcast.43.refs_1_.refs_2_), slice={[0:512], [2048:2688]} | slice | bytes 1310720 | tf_op jit(solution)/shard_map/slice | solution.py:477
  56.8 5.4 %expert_rows.2 = bf16[512,2048]{1,0:T(8,128)(2,1)} custom-call(s32[1]{0:T(128)} %bitcast.42.refs_0_, bf16[512,2688]{1,0:T(8,128)(2,1)} %bitcast.43.refs_1_.refs_2_, bf16[512,2688]{1,0:T(8,128)(2,1)} %bitcast.43.refs_1_.refs_2_, bf16[2048,256]{1,0:T(8,128)(2,1)} %bitcast.130, bf16[2048,256]{1,0:T(8,128)(2,1)} %bitcast.132, bf16[256,2048]{1,0:T(8,128)(2,1)} %bitcast.134), custom_call_target="tpu_custom_call" | custom-call | flops 1610612736 | bytes 7340032 | tf_op jit(solution)/shard_map/expert_rows/pallas_call | solution.py:251
  62.2 2.0 %slice.85 = bf16[512,640]{1,0:T(8,128)(2,1)} slice(bf16[512,2688]{1,0:T(8,128)(2,1)} %collective-permute-done.7.refs_1_.refs_2_), slice={[0:512], [2048:2688]} | slice | bytes 1310720 | tf_op jit(solution)/shard_map/slice | solution.py:477
  64.2 5.4 %expert_rows.3 = bf16[512,2048]{1,0:T(8,128)(2,1)} custom-call(s32[1]{0:T(128)} %bitcast.42.refs_0_, bf16[512,2688]{1,0:T(8,128)(2,1)} %collective-permute-done.7.refs_1_.refs_2_, bf16[512,2688]{1,0:T(8,128)(2,1)} %collective-permute-done.7.refs_1_.refs_2_, bf16[2048,256]{1,0:T(8,128)(2,1)} %bitcast.131, bf16[2048,256]{1,0:T(8,128)(2,1)} %bitcast.133, ...), custom_call_target="tpu_custom_call" | custom-call | flops 1610612736 | bytes 7340032 | tf_op jit(solution)/shard_map/expert_rows/pallas_call | solution.py:251
  73.0 1.8 %convolution_convert_fusion = bf16[1024,512]{0,1:T(8,128)(2,1)} fusion(bf16[512,512]{1,0:T(8,128)(2,1)S(1)} %copy-done.6, bf16[1024,640]{1,0:T(8,128)(2,1)S(1)} %constant_dynamic-update-slice_fusion.5), kind=kOutput, calls=%fused_computation.7 | convolution fusion | flops 537395200 | bytes 2621440 | tf_op jit(solution)/shard_map/dot_general | solution.py:495
  76.4 2.4 %add_convert_fusion = bf16[512,2048]{1,0:T(8,128)(2,1)S(1)} fusion(bf16[512,2048]{1,0:T(8,128)(2,1)} %collective-permute-done.8, bf16[512,2048]{1,0:T(8,128)(2,1)S(1)} %copy-done.2), kind=kLoop, calls=%fused_computation | loop fusion | flops 4194304 | bytes 6291456 | tf_op jit(solution)/shard_map/convert_element_type | solution.py:387
  80.5 1.8 %fusion.26 = (f32[4,128]{1,0:T(4,128)S(1)}, bf16[4,128,1024]{2,1,0:T(8,128)(2,1)}) fusion(f32[4,128,1024]{2,1,0:T(8,128)S(1)} %fusion.27, bf16[128,4,64]{0,2,1:T(8,128)(2,1)S(1)} %pad_maximum_fusion.3, bf16[1024,64]{1,0:T(8,128)(2,1)S(1)} %slice.112, pred[128,1024]{1,0:T(8,128)(4,1)S(1)} %broadcast_compare_fusion), kind=kOutput, calls=%fused_computation.81 | convolution fusion | flops 69729792 | bytes 3475456 | tf_op jit(solution)/shard_map/ihd,jd->hij/dot_general | solution.py:520
  82.3 3.8 %fusion = bf16[128,2048]{1,0:T(8,128)(2,1)} fusion(bf16[4,128,2048]{2,1,0:T(8,128)(2,1)} %bitcast.151, bf16[4,128,1024]{2,1,0:T(8,128)(2,1)} %bitcast.152, bf16[4,128,1024]{2,1,0:T(8,128)(2,1)} %get-tuple-element.43, f32[4,128]{1,0:T(4,128)S(1)} %get-tuple-element.42), kind=kOutput, calls=%fused_computation.2 | convolution fusion | flops 403046400 | bytes 4720640 | tf_op jit(solution)/shard_map/hid,hde->ie/dot_general | solution.py:534
  87.2 1.6 %collective-permute-start.11 = (bf16[2,2,32,2048]{3,2,1,0:T(8,128)(2,1)}, bf16[2,2,32,2048]{3,2,1,0:T(8,128)(2,1)S(1)}, u32[]{:S(2)}, u32[]{:S(2)}) collective-permute-start(bf16[2,2,32,2048]{3,2,1,0:T(8,128)(2,1)} %get-tuple-element.26), channel_id=1, source_target_pairs={{0,4},{4,0},{8,12},{12,8},{16,20},{20,16},{24,28},{28,24},{1,5},{5... | collective-permute-start | bytes 1572872 | tf_op jit(solution)/shard_map/ppermute | solution.py:422
  90.3 1.6 %collective-permute-start.10 = (bf16[32,2048]{1,0:T(8,128)(2,1)S(1)}, bf16[32,2048]{1,0:T(8,128)(2,1)S(1)}, u32[]{:S(2)}, u32[]{:S(2)}) collective-permute-start(bf16[32,2048]{1,0:T(8,128)(2,1)S(1)} %slice_bitcast_fusion.10), channel_id=1, source_target_pairs={{0,2},{1,3},{2,0},{3,1},{4,6},{5,7},{6,4},{7,5},{8,10},{9,11},{10,... | collective-permute-start | bytes 393224 | tf_op jit(solution)/shard_map/ppermute | solution.py:422
  91.9 13.9 %collective-permute-done.10 = bf16[32,2048]{1,0:T(8,128)(2,1)S(1)} collective-permute-done((bf16[32,2048]{1,0:T(8,128)(2,1)S(1)}, bf16[32,2048]{1,0:T(8,128)(2,1)S(1)}, u32[]{:S(2)}, u32[]{:S(2)}) %collective-permute-start.10) | collective-permute-done | bytes 131104 | tf_op jit(solution)/shard_map/ppermute | solution.py:422
  105.9 1.6 %add_convert_fusion.2 = (bf16[2,2,32,2048]{3,2,1,0:T(8,128)(2,1)S(1)}, bf16[2,2,32,2048]{3,2,1,0:T(8,128)(2,1)S(1)}) fusion(bf16[2,2,32,2048]{3,2,1,0:T(8,128)(2,1)S(1)} %collective-permute-done.11, bf16[4,4,32,2048]{3,2,1,0:T(8,128)(2,1)} %bitcast.129, bf16[2,2,32,2048]{3,2,1,0:T(8,128)(2,1)S(1)} %collective-permute-done.14), kind=kLoop, calls=%fused_computation.17 | loop fusion | flops 2097152 | bytes 3145728 | tf_op jit(solution)/shard_map/convert_element_type | solution.py:387
  109.4 5.8 %collective-permute-done.15 = bf16[2,32,2048]{2,1,0:T(8,128)(2,1)S(1)} collective-permute-done((bf16[2,32,2048]{2,1,0:T(8,128)(2,1)S(1)}, bf16[2,32,2048]{2,1,0:T(8,128)(2,1)S(1)}, u32[]{:S(2)}, u32[]{:S(2)}) %collective-permute-start.15) | collective-permute-done | bytes 262176 | tf_op jit(solution)/shard_map/ppermute | solution.py:422
  115.3 2.2 %collective-permute-start.17 = (bf16[32,2048]{1,0:T(8,128)(2,1)S(1)}, bf16[32,2048]{1,0:T(8,128)(2,1)S(1)}, u32[]{:S(2)}, u32[]{:S(2)}) collective-permute-start(bf16[32,2048]{1,0:T(8,128)(2,1)S(1)} %get-tuple-element.39), channel_id=1, source_target_pairs={{0,24},{4,28},{8,16},{12,20},{16,8},{20,12},{24,0},{28,4},{1,25},{... | collective-permute-start | bytes 393224 | tf_op jit(solution)/shard_map/ppermute | solution.py:422
  119.7 5.5 %collective-permute-done.16 = bf16[32,2048]{1,0:T(8,128)(2,1)S(1)} collective-permute-done((bf16[32,2048]{1,0:T(8,128)(2,1)S(1)}, bf16[32,2048]{1,0:T(8,128)(2,1)S(1)}, u32[]{:S(2)}, u32[]{:S(2)}) %collective-permute-start.16) | collective-permute-done | bytes 131104 | tf_op jit(solution)/shard_map/ppermute | solution.py:422
  (84 shorter events, 27.4 us)
Async XLA Ops:
  0.6 12.6 %copy-start = (bf16[2048,768]{1,0:T(8,128)(2,1)S(1)}, bf16[2048,768]{1,0:T(8,128)(2,1)}, u32[]{:S(2)}) copy-start(bf16[2048,768]{1,0:T(8,128)(2,1)} %param.19) | copy-start | bytes 9437188
  1.9 11.3 %copy-start.4 = (f32[2048]{0:T(1024)S(1)}, f32[2048]{0:T(1024)}, u32[]{:S(2)}) copy-start(f32[2048]{0:T(1024)} %param.18) | copy-start | bytes 24580
  5.9 10.6 %collective-permute-start.2 = (bf16[1,32,2688]{2,1,0:T(8,128)(2,1)}, bf16[1,32,2688]{2,1,0:T(8,128)(2,1)S(1)}, u32[]{:S(2)}, u32[]{:S(2)}) collective-permute-start(bf16[1,32,2688]{2,1,0:T(8,128)(2,1)} %bitcast.137), channel_id=1, source_target_pairs={{0,24},{4,28},{8,16},{12,20},{16,8},{20,12},{24,0},{28,4},{1,25},{... | collective-permute-start | bytes 516104 | tf_op jit(solution)/shard_map/ppermute | solution.py:422
  10.9 14.9 %collective-permute-start.1 = (bf16[1,32,2688]{2,1,0:T(8,128)(2,1)}, bf16[1,32,2688]{2,1,0:T(8,128)(2,1)}, u32[]{:S(2)}, u32[]{:S(2)}) collective-permute-start(bf16[1,32,2688]{2,1,0:T(8,128)(2,1)} %bitcast.138), channel_id=1, source_target_pairs={{0,16},{4,20},{8,24},{12,28},{16,0},{20,4},{24,8},{28,12},{1,17},{... | collective-permute-start | bytes 516104 | tf_op jit(solution)/shard_map/ppermute | solution.py:422
  10.9 14.9 %collective-permute-start = (bf16[1,32,2688]{2,1,0:T(8,128)(2,1)}, bf16[1,32,2688]{2,1,0:T(8,128)(2,1)}, u32[]{:S(2)}, u32[]{:S(2)}) collective-permute-start(bf16[1,32,2688]{2,1,0:T(8,128)(2,1)} %bitcast.139), channel_id=1, source_target_pairs={{0,8},{4,12},{8,0},{12,4},{16,24},{20,28},{24,16},{28,20},{1,9},{5... | collective-permute-start | bytes 516104 | tf_op jit(solution)/shard_map/ppermute | solution.py:422
  13.2 12.6 %copy-start.3 = (bf16[32,2688]{1,0:T(8,128)(2,1)S(1)}, bf16[32,2688]{1,0:T(8,128)(2,1)}, u32[]{:S(2)}) copy-start(bf16[32,2688]{1,0:T(8,128)(2,1)} %own_rows.1) | copy-start | bytes 516100
  27.0 16.6 %collective-permute-start.4 = (bf16[4,32,2688]{2,1,0:T(8,128)(2,1)S(1)}, bf16[4,32,2688]{2,1,0:T(8,128)(2,1)S(1)}, u32[]{:S(2)}, u32[]{:S(2)}) collective-permute-start(bf16[4,32,2688]{2,1,0:T(8,128)(2,1)S(1)} %pad_maximum_fusion), channel_id=1, source_target_pairs={{0,4},{4,0},{8,12},{12,8},{16,20},{20,16},{24,28},{28,24},{1,5},{5... | collective-permute-start | bytes 2064392 | tf_op jit(solution)/shard_map/ppermute | solution.py:422
  28.5 16.6 %collective-permute-start.3 = (bf16[4,32,2688]{2,1,0:T(8,128)(2,1)S(1)}, bf16[4,32,2688]{2,1,0:T(8,128)(2,1)S(1)}, u32[]{:S(2)}, u32[]{:S(2)}) collective-permute-start(bf16[4,32,2688]{2,1,0:T(8,128)(2,1)S(1)} %pad_maximum_fusion), channel_id=1, source_target_pairs={{0,2},{1,3},{2,0},{3,1},{4,6},{5,7},{6,4},{7,5},{8,10},{9,11},{10,... | collective-permute-start | bytes 2064392 | tf_op jit(solution)/shard_map/ppermute | solution.py:422
  43.6 10.4 %collective-permute-start.6 = (bf16[2,32,2688]{2,1,0:T(8,128)(2,1)S(1)}, bf16[2,32,2688]{2,1,0:T(8,128)(2,1)S(1)}, u32[]{:S(2)}, u32[]{:S(2)}) collective-permute-start(bf16[2,32,2688]{2,1,0:T(8,128)(2,1)S(1)} %slice.108), channel_id=1, source_target_pairs={{0,2},{1,3},{2,0},{3,1},{4,6},{5,7},{6,4},{7,5},{8,10},{9,11},{10,... | collective-permute-start | bytes 1032200 | tf_op jit(solution)/shard_map/ppermute | solution.py:422
  45.2 8.1 %collective-permute-start.5 = (bf16[2,32,2688]{2,1,0:T(8,128)(2,1)S(1)}, bf16[2,32,2688]{2,1,0:T(8,128)(2,1)S(1)}, u32[]{:S(2)}, u32[]{:S(2)}) collective-permute-start(bf16[2,32,2688]{2,1,0:T(8,128)(2,1)S(1)} %slice.107), channel_id=1, source_target_pairs={{0,4},{4,0},{8,12},{12,8},{16,20},{20,16},{24,28},{28,24},{1,5},{5... | collective-permute-start | bytes 1032200 | tf_op jit(solution)/shard_map/ppermute | solution.py:422
  54.8 7.5 %collective-permute-start.7 = (bf16[512,2688]{1,0:T(8,128)(2,1)}, bf16[512,2688]{1,0:T(8,128)(2,1)}, u32[]{:S(2)}, u32[]{:S(2)}) collective-permute-start(bf16[512,2688]{1,0:T(8,128)(2,1)} %bitcast.43.refs_1_.refs_2_), channel_id=1, source_target_pairs={{0,1},{1,0},{2,3},{3,2},{4,5},{5,4},{6,7},{7,6},{8,9},{9,8},{10,11... | collective-permute-start | bytes 8257544 | tf_op jit(solution)/shard_map/ppermute | solution.py:422
  69.6 6.0 %collective-permute-start.8 = (bf16[512,2048]{1,0:T(8,128)(2,1)}, bf16[512,2048]{1,0:T(8,128)(2,1)}, u32[]{:S(2)}, u32[]{:S(2)}) collective-permute-start(bf16[512,2048]{1,0:T(8,128)(2,1)} %expert_rows.3), channel_id=1, source_target_pairs={{0,1},{1,0},{2,3},{3,2},{4,5},{5,4},{6,7},{7,6},{8,9},{9,8},{10,11... | collective-permute-start | bytes 6291464 | tf_op jit(solution)/shard_map/ppermute | solution.py:422
  70.4 2.6 %copy-start.6 = (bf16[512,512]{1,0:T(8,128)(2,1)S(1)}, bf16[512,512]{1,0:T(8,128)(2,1)}, u32[]{:S(2)}) copy-start(bf16[512,512]{1,0:T(8,128)(2,1)} %param.24) | copy-start | bytes 1572868
  71.7 3.1 %copy-start.7 = (bf16[512,512]{1,0:T(8,128)(2,1)S(1)}, bf16[512,512]{1,0:T(8,128)(2,1)}, u32[]{:S(2)}) copy-start(bf16[512,512]{1,0:T(8,128)(2,1)} %param.23) | copy-start | bytes 1572868
  87.1 2.1 %collective-permute-start.9 = (bf16[2,32,2048]{2,1,0:T(8,128)(2,1)S(1)}, bf16[2,32,2048]{2,1,0:T(8,128)(2,1)S(1)}, u32[]{:S(2)}, u32[]{:S(2)}) collective-permute-start(bf16[2,32,2048]{2,1,0:T(8,128)(2,1)S(1)} %slice_bitcast_fusion.4), channel_id=1, source_target_pairs={{0,1},{1,0},{2,3},{3,2},{4,5},{5,4},{6,7},{7,6},{8,9},{9,8},{10,11... | collective-permute-start | bytes 786440 | tf_op jit(solution)/shard_map/ppermute | solution.py:422
  87.2 18.7 %collective-permute-start.11 = (bf16[2,2,32,2048]{3,2,1,0:T(8,128)(2,1)}, bf16[2,2,32,2048]{3,2,1,0:T(8,128)(2,1)S(1)}, u32[]{:S(2)}, u32[]{:S(2)}) collective-permute-start(bf16[2,2,32,2048]{3,2,1,0:T(8,128)(2,1)} %get-tuple-element.26), channel_id=1, source_target_pairs={{0,4},{4,0},{8,12},{12,8},{16,20},{20,16},{24,28},{28,24},{1,5},{5... | collective-permute-start | bytes 1572872 | tf_op jit(solution)/shard_map/ppermute | solution.py:422
  88.7 17.2 %collective-permute-start.14 = (bf16[2,2,32,2048]{3,2,1,0:T(8,128)(2,1)}, bf16[2,2,32,2048]{3,2,1,0:T(8,128)(2,1)S(1)}, u32[]{:S(2)}, u32[]{:S(2)}) collective-permute-start(bf16[2,2,32,2048]{3,2,1,0:T(8,128)(2,1)} %get-tuple-element.27), channel_id=1, source_target_pairs={{0,2},{1,3},{2,0},{3,1},{4,6},{5,7},{6,4},{7,5},{8,10},{9,11},{10,... | collective-permute-start | bytes 1572872 | tf_op jit(solution)/shard_map/ppermute | solution.py:422
  90.3 15.5 %collective-permute-start.10 = (bf16[32,2048]{1,0:T(8,128)(2,1)S(1)}, bf16[32,2048]{1,0:T(8,128)(2,1)S(1)}, u32[]{:S(2)}, u32[]{:S(2)}) collective-permute-start(bf16[32,2048]{1,0:T(8,128)(2,1)S(1)} %slice_bitcast_fusion.10), channel_id=1, source_target_pairs={{0,2},{1,3},{2,0},{3,1},{4,6},{5,7},{6,4},{7,5},{8,10},{9,11},{10,... | collective-permute-start | bytes 393224 | tf_op jit(solution)/shard_map/ppermute | solution.py:422
  107.5 11.4 %copy-start.5 = (f32[2048]{0:T(1024)S(1)}, f32[2048]{0:T(1024)}, u32[]{:S(2)}) copy-start(f32[2048]{0:T(1024)} %param.26) | copy-start | bytes 24580
  107.6 7.6 %collective-permute-start.15 = (bf16[2,32,2048]{2,1,0:T(8,128)(2,1)S(1)}, bf16[2,32,2048]{2,1,0:T(8,128)(2,1)S(1)}, u32[]{:S(2)}, u32[]{:S(2)}) collective-permute-start(bf16[2,32,2048]{2,1,0:T(8,128)(2,1)S(1)} %slice_bitcast_fusion), channel_id=1, source_target_pairs={{0,4},{4,0},{8,12},{12,8},{16,20},{20,16},{24,28},{28,24},{1,5},{5... | collective-permute-start | bytes 786440 | tf_op jit(solution)/shard_map/ppermute | solution.py:422
  108.2 9.3 %collective-permute-start.12 = (bf16[2,32,2048]{2,1,0:T(8,128)(2,1)S(1)}, bf16[2,32,2048]{2,1,0:T(8,128)(2,1)S(1)}, u32[]{:S(2)}, u32[]{:S(2)}) collective-permute-start(bf16[2,32,2048]{2,1,0:T(8,128)(2,1)S(1)} %slice_bitcast_fusion.2), channel_id=1, source_target_pairs={{0,2},{1,3},{2,0},{3,1},{4,6},{5,7},{6,4},{7,5},{8,10},{9,11},{10,... | collective-permute-start | bytes 786440 | tf_op jit(solution)/shard_map/ppermute | solution.py:422
  115.2 10.0 %collective-permute-start.16 = (bf16[32,2048]{1,0:T(8,128)(2,1)S(1)}, bf16[32,2048]{1,0:T(8,128)(2,1)S(1)}, u32[]{:S(2)}, u32[]{:S(2)}) collective-permute-start(bf16[32,2048]{1,0:T(8,128)(2,1)S(1)} %get-tuple-element.38), channel_id=1, source_target_pairs={{0,16},{4,20},{8,24},{12,28},{16,0},{20,4},{24,8},{28,12},{1,17},{... | collective-permute-start | bytes 393224 | tf_op jit(solution)/shard_map/ppermute | solution.py:422
  115.3 9.9 %collective-permute-start.17 = (bf16[32,2048]{1,0:T(8,128)(2,1)S(1)}, bf16[32,2048]{1,0:T(8,128)(2,1)S(1)}, u32[]{:S(2)}, u32[]{:S(2)}) collective-permute-start(bf16[32,2048]{1,0:T(8,128)(2,1)S(1)} %get-tuple-element.39), channel_id=1, source_target_pairs={{0,24},{4,28},{8,16},{12,20},{16,8},{20,12},{24,0},{28,4},{1,25},{... | collective-permute-start | bytes 393224 | tf_op jit(solution)/shard_map/ppermute | solution.py:422
  117.6 9.0 %collective-permute-start.13 = (bf16[32,2048]{1,0:T(8,128)(2,1)S(1)}, bf16[32,2048]{1,0:T(8,128)(2,1)S(1)}, u32[]{:S(2)}, u32[]{:S(2)}) collective-permute-start(bf16[32,2048]{1,0:T(8,128)(2,1)S(1)} %slice_bitcast_fusion.8), channel_id=1, source_target_pairs={{0,8},{4,12},{8,0},{12,4},{16,24},{20,28},{24,16},{28,20},{1,9},{5... | collective-permute-start | bytes 393224 | tf_op jit(solution)/shard_map/ppermute | solution.py:422
  (2 other events, 3.3 us)

commit v3 on v2

--- a/solution.py
+++ b/solution.py
@@ -214,6 +214,7 @@
     own_gates = lax.dynamic_slice_in_dim(gate_share, tp_index * quarter_rows, quarter_rows, 0)
     moe_out = jnp.sum(picked * own_gates[:, :, None], axis=1).astype(jnp.bfloat16)
     return (mixed, moe_out)
+
 
 LANES = 128
 
@@ -473,13 +474,9 @@
     near_out, far = lax.optimization_barrier((near_out, far))
     far_out = apply_expert(expert, far, *weights_of, latent_width, experts)
 
-    far_out, near_kept, far_kept = lax.optimization_barrier(
-        (far_out, near[:, width:], far[:, width:])
-    )
-
-    kept = jnp.concatenate([near_kept, far_kept], axis=0)
-    latents = kept[:, :latent_width]
-    turns = kept[:, latent_width : latent_width + ROPE]
+    far_out, near, far = lax.optimization_barrier((far_out, near, far))
+
+    kept = jnp.concatenate([near[:, width:], far[:, width:]], axis=0)
     places = []
     for core in (0, 1):
         for x_bit, y_bit in ((0, 0), (0, 2), (1, 0), (1, 2)):
@@ -488,6 +485,27 @@
                     (ep_index ^ (2 * k + x_bit)) * row_count + (tp_index ^ (y_bit + core)) * piece
                 )
     key_places = (jnp.stack(places)[:, None] + steps[None, :]).reshape(-1)
+
+    blocks = add_pieces(near_out, swap(far_out, "tp", 1)).reshape(4, lines, piece, width)
+    sent_x, sent_y, kept = lax.optimization_barrier(
+        (blocks[2:, :half], blocks[1::2, half:], kept)
+    )
+    got_x = swap(sent_x, "ep", 1)
+    got_y = swap(sent_y, "tp", 2)
+    first = add_pieces(blocks[:2, :half], got_x)
+    second = add_pieces(blocks[0::2, half:], got_y)
+    got_y = swap(first[1], "tp", 2)
+    got_x = swap(second[1], "ep", 1)
+    summed = jnp.concatenate(
+        [add_pieces(first[0], got_y), add_pieces(second[0], got_x)], axis=0
+    )
+    moe_sum = summed[0].astype(jnp.float32)
+    for k in range(1, lines):
+        moe_sum = moe_sum + swap(summed[k], "ep", 2 * k).astype(jnp.float32)
+    moe_out = moe_sum.astype(jnp.bfloat16)
+
+    latents = kept[:, :latent_width]
+    turns = kept[:, latent_width : latent_width + ROPE]
     contract = (((0,), (1,)), ((), ()))
     key_block = lax.dot_general(
         key_weight, latents, contract, preferred_element_type=jnp.float32
@@ -498,24 +516,6 @@
     key_count = key_block.shape[1]
     key_block = key_block.reshape(head_count, NOPE, key_count)
     value_block = value_block.reshape(head_count, VD, key_count)
-    blocks = add_pieces(near_out, swap(far_out, "tp", 1)).reshape(4, lines, piece, width)
-    sent_x, sent_y, key_block, value_block, turns = lax.optimization_barrier(
-        (blocks[2:, :half], blocks[1::2, half:], key_block, value_block, turns)
-    )
-    got_x = swap(sent_x, "ep", 1)
-    got_y = swap(sent_y, "tp", 2)
-    first = add_pieces(blocks[:2, :half], got_x)
-    second = add_pieces(blocks[0::2, half:], got_y)
-    got_y = swap(first[1], "tp", 2)
-    got_x = swap(second[1], "ep", 1)
-    summed = jnp.concatenate(
-        [add_pieces(first[0], got_y), add_pieces(second[0], got_x)], axis=0
-    )
-    moe_sum = summed[0].astype(jnp.float32)
-    for k in range(1, lines):
-        moe_sum = moe_sum + swap(summed[k], "ep", 2 * k).astype(jnp.float32)
-    moe_out = moe_sum.astype(jnp.bfloat16)
-
     scores = jnp.einsum("ihd,hdj->hij", query_plain, key_block, preferred_element_type=jnp.float32)
     scores = scores + jnp.einsum(
         "ihd,jd->hij", query_turn, turns, preferred_element_type=jnp.float32

time: 128 us -> 124 us (0.969)
  local copies, waits for them, and re-layouts: 15.3 us -> 11.3 us
  waiting for transfers between devices: 54.9 us -> 52.9 us
  other arithmetic: 9.75 us -> 11.1 us
    ppermute x18, waiting for transfers between devices: 54.9 us -> 52.9 us  [swap(): return lax.ppermute(array, axis, [(i, i ^ bit) for i in range(size)])]
    slice x3 -> x2, local copies, waits for them, and re-layouts: 4.09 us -> 2.44 us  [local_dense(): kept = jnp.concatenate([near[:, width:], far[:, width:]], axis=0)]
    unnamed x21 -> x24, local copies, waits for them, and re-layouts: 5.58 us -> 4.52 us
  transfers between devices with their start and end apart: 18 -> 18, of which waited for: 8 -> 10; matrix products, arithmetic and copies ran while one was open for 13% -> 11% of each run, Pallas kernels for 4% -> 4%
where the time goes in v3:
time: 124 us
  waiting for transfers between devices  52.9 us (43%)
  starting transfers between devices  22.1 us (18%)
  Pallas kernels  14.7 us (12%)
  local copies, waits for them, and re-layouts  11.3 us (9%)
  other arithmetic  11.1 us (9%)
  matrix products  10.9 us (9%)
    ppermute x18, waiting for transfers between devices, swap(): return lax.ppermute(array, axis, [(i, i ^ bit) for i in range(size)])  52.9 us
    ppermute x18, starting transfers between devices, swap(): return lax.ppermute(array, axis, [(i, i ^ bit) for i in range(size)])  22.1 us
    pallas_call x2, Pallas kernels, apply_expert(): pl.pallas_call(lambda *refs: expert_rows(*refs, experts=experts), grid=(c...  10.8 us
    convert_element_type x5, other arithmetic, add_pieces(): (left.astype(jnp.float32) + right.astype(jnp.float32)).astype(jnp.bfloat16)  5.1 us
    unnamed x24, local copies, waits for them, and re-layouts  4.52 us
    pallas_call x1, Pallas kernels, own_piece(): pl.pallas_call(lambda *refs: own_rows(*refs, piece=piece, experts=experts...  3.98 us
    dot_general x1, matrix products, local_dense(): jnp.einsum('hid,hde->ie', attended, mixing, preferred_element_type=jnp.fl...  3.84 us
  transfers between devices with their start and end apart: 18, of which 10 were waited for; matrix products, arithmetic and copies ran while one was open for 11% of the time, Pallas kernels for 4%

profile of v3, /device:TPU:0, one launch (start us, length us, event | category | flops | bytes accessed | tf_op | source)
XLA Modules:
  0.0 124.0 jit_solution(5001558959434668786)
XLA Ops:
  1.9 4.0 %own_rows.1 = bf16[32,2688]{1,0:T(8,128)(2,1)} custom-call(s32[2]{0:T(128)} %pad_add_fusion.refs_0_, bf16[128,2048]{1,0:T(8,128)(2,1)} %refs_1_.1, f32[1,2048]{1,0:T(1,128)} %bitcast.146, bf16[128,2048]{1,0:T(8,128)(2,1)} %refs_3_.1, f32[1,2048]{1,0:T(1,128)} %bitcast.147, bf16[2048,512]{1,0:T(8,128)(2,1)} %refs_5_.1, f32[1,512]{1,0:T(1,128)} %bitcast.148, ...), custom_call_target="tpu_custom_call" | custom-call | tf_op jit(solution)/shard_map/own_rows/pallas_call | solution.py:373
  5.9 3.1 %collective-permute-start = (bf16[1,32,2688]{2,1,0:T(8,128)(2,1)}, bf16[1,32,2688]{2,1,0:T(8,128)(2,1)}, u32[]{:S(2)}, u32[]{:S(2)}) collective-permute-start(bf16[1,32,2688]{2,1,0:T(8,128)(2,1)} %bitcast.137), channel_id=1, source_target_pairs={{0,8},{4,12},{8,0},{12,4},{16,24},{20,28},{24,16},{28,20},{1,9},{5... | collective-permute-start | bytes 516104 | tf_op jit(solution)/shard_map/ppermute | solution.py:423
  8.9 2.6 %collective-permute-start.1 = (bf16[1,32,2688]{2,1,0:T(8,128)(2,1)}, bf16[1,32,2688]{2,1,0:T(8,128)(2,1)}, u32[]{:S(2)}, u32[]{:S(2)}) collective-permute-start(bf16[1,32,2688]{2,1,0:T(8,128)(2,1)} %bitcast.138), channel_id=1, source_target_pairs={{0,16},{4,20},{8,24},{12,28},{16,0},{20,4},{24,8},{28,12},{1,17},{... | collective-permute-start | bytes 516104 | tf_op jit(solution)/shard_map/ppermute | solution.py:423
  15.1 2.3 %fusion.12 = f32[128,768]{0,1:T(8,128)S(1)} fusion(bf16[2048,768]{1,0:T(8,128)(2,1)S(1)} %copy-done, f32[2048]{0:T(1024)S(1)} %copy-done.5, f32[128]{0:T(128)} %add_rsqrt_fusion.1, bf16[32,2048]{1,0:T(8,128)(2,1)S(1)} %get-tuple-element.30, bf16[32,2048]{1,0:T(8,128)(2,1)} %copy-done.4, bf16[32,2048]{1,0:T(8,128)(2,1)S(1)} %get-tuple-element.29, ...), kind=kOutput, calls=%fused_computation.23 | convolution fusion | flops 405536768 | bytes 4071936 | tf_op jit(solution)/shard_map/dot_general | solution.py:453
  17.5 7.3 %collective-permute-done.1 = bf16[1,32,2688]{2,1,0:T(8,128)(2,1)} collective-permute-done((bf16[1,32,2688]{2,1,0:T(8,128)(2,1)}, bf16[1,32,2688]{2,1,0:T(8,128)(2,1)}, u32[]{:S(2)}, u32[]{:S(2)}) %collective-permute-start.1) | collective-permute-done | bytes 172064 | tf_op jit(solution)/shard_map/ppermute | solution.py:423
  26.0 1.6 %collective-permute-start.3 = (bf16[4,32,2688]{2,1,0:T(8,128)(2,1)S(1)}, bf16[4,32,2688]{2,1,0:T(8,128)(2,1)S(1)}, u32[]{:S(2)}, u32[]{:S(2)}) collective-permute-start(bf16[4,32,2688]{2,1,0:T(8,128)(2,1)S(1)} %pad_maximum_fusion.1), channel_id=1, source_target_pairs={{0,2},{1,3},{2,0},{3,1},{4,6},{5,7},{6,4},{7,5},{8,10},{9,11},{10,... | collective-permute-start | bytes 2064392 | tf_op jit(solution)/shard_map/ppermute | solution.py:423
  27.6 1.5 %collective-permute-start.4 = (bf16[4,32,2688]{2,1,0:T(8,128)(2,1)S(1)}, bf16[4,32,2688]{2,1,0:T(8,128)(2,1)S(1)}, u32[]{:S(2)}, u32[]{:S(2)}) collective-permute-start(bf16[4,32,2688]{2,1,0:T(8,128)(2,1)S(1)} %pad_maximum_fusion.1), channel_id=1, source_target_pairs={{0,4},{4,0},{8,12},{12,8},{16,20},{20,16},{24,28},{28,24},{1,5},{5... | collective-permute-start | bytes 2064392 | tf_op jit(solution)/shard_map/ppermute | solution.py:423
  30.0 10.8 %collective-permute-done.3 = bf16[4,32,2688]{2,1,0:T(8,128)(2,1)S(1)} collective-permute-done((bf16[4,32,2688]{2,1,0:T(8,128)(2,1)S(1)}, bf16[4,32,2688]{2,1,0:T(8,128)(2,1)S(1)}, u32[]{:S(2)}, u32[]{:S(2)}) %collective-permute-start.3) | collective-permute-done | bytes 688160 | tf_op jit(solution)/shard_map/ppermute | solution.py:423
  40.8 1.6 %collective-permute-start.5 = (bf16[2,32,2688]{2,1,0:T(8,128)(2,1)S(1)}, bf16[2,32,2688]{2,1,0:T(8,128)(2,1)S(1)}, u32[]{:S(2)}, u32[]{:S(2)}) collective-permute-start(bf16[2,32,2688]{2,1,0:T(8,128)(2,1)S(1)} %slice.107), channel_id=1, source_target_pairs={{0,4},{4,0},{8,12},{12,8},{16,20},{20,16},{24,28},{28,24},{1,5},{5... | collective-permute-start | bytes 1032200 | tf_op jit(solution)/shard_map/ppermute | solution.py:423
  42.4 1.7 %collective-permute-done.4 = bf16[4,32,2688]{2,1,0:T(8,128)(2,1)S(1)} collective-permute-done((bf16[4,32,2688]{2,1,0:T(8,128)(2,1)S(1)}, bf16[4,32,2688]{2,1,0:T(8,128)(2,1)S(1)}, u32[]{:S(2)}, u32[]{:S(2)}) %collective-permute-start.4) | collective-permute-done | bytes 688160 | tf_op jit(solution)/shard_map/ppermute | solution.py:423
  46.2 3.2 %collective-permute-done.5 = bf16[2,32,2688]{2,1,0:T(8,128)(2,1)S(1)} collective-permute-done((bf16[2,32,2688]{2,1,0:T(8,128)(2,1)S(1)}, bf16[2,32,2688]{2,1,0:T(8,128)(2,1)S(1)}, u32[]{:S(2)}, u32[]{:S(2)}) %collective-permute-start.5) | collective-permute-done | bytes 344096 | tf_op jit(solution)/shard_map/ppermute | solution.py:423
  52.2 5.4 %expert_rows.2 = bf16[512,2048]{1,0:T(8,128)(2,1)} custom-call(s32[1]{0:T(128)} %bitcast.42.refs_0_, bf16[512,2688]{1,0:T(8,128)(2,1)} %bitcast.43.refs_1_.refs_2_, bf16[512,2688]{1,0:T(8,128)(2,1)} %bitcast.43.refs_1_.refs_2_, bf16[2048,256]{1,0:T(8,128)(2,1)} %bitcast.130, bf16[2048,256]{1,0:T(8,128)(2,1)} %bitcast.132, bf16[256,2048]{1,0:T(8,128)(2,1)} %bitcast.134), custom_call_target="tpu_custom_call" | custom-call | flops 1610612736 | bytes 7340032 | tf_op jit(solution)/shard_map/expert_rows/pallas_call | solution.py:252
  57.6 5.4 %expert_rows.3 = bf16[512,2048]{1,0:T(8,128)(2,1)} custom-call(s32[1]{0:T(128)} %bitcast.42.refs_0_, bf16[512,2688]{1,0:T(8,128)(2,1)} %collective-permute-done.7.refs_1_.refs_2_, bf16[512,2688]{1,0:T(8,128)(2,1)} %collective-permute-done.7.refs_1_.refs_2_, bf16[2048,256]{1,0:T(8,128)(2,1)} %bitcast.131, bf16[2048,256]{1,0:T(8,128)(2,1)} %bitcast.133, ...), custom_call_target="tpu_custom_call" | custom-call | flops 1610612736 | bytes 7340032 | tf_op jit(solution)/shard_map/expert_rows/pallas_call | solution.py:252
  67.6 2.4 %add_convert_fusion = bf16[512,2048]{1,0:T(8,128)(2,1)S(1)} fusion(bf16[512,2048]{1,0:T(8,128)(2,1)} %collective-permute-done.8, bf16[512,2048]{1,0:T(8,128)(2,1)S(1)} %copy-done.2), kind=kLoop, calls=%fused_computation | loop fusion | flops 4194304 | bytes 6291456 | tf_op jit(solution)/shard_map/convert_element_type | solution.py:388
  72.2 1.7 %convolution_convert_fusion = bf16[1024,512]{0,1:T(8,128)(2,1)} fusion(bf16[512,512]{1,0:T(8,128)(2,1)S(1)} %copy-done.9, bf16[1024,640]{1,0:T(8,128)(2,1)S(1)} %pad_maximum_fusion), kind=kOutput, calls=%fused_computation.7 | convolution fusion | flops 537395200 | bytes 2621440 | tf_op jit(solution)/shard_map/dot_general | solution.py:513
  74.4 1.8 %fusion.27 = (f32[4,128]{1,0:T(4,128)S(1)}, bf16[4,128,1024]{2,1,0:T(8,128)(2,1)}) fusion(f32[4,128,1024]{2,1,0:T(8,128)S(1)} %fusion.28, bf16[128,4,64]{0,2,1:T(8,128)(2,1)S(1)} %pad_maximum_fusion.4, bf16[1024,640]{1,0:T(8,128)(2,1)S(1)} %pad_maximum_fusion, pred[128,1024]{1,0:T(8,128)(4,1)S(1)} %broadcast_compare_fusion), kind=kOutput, calls=%fused_computation.81 | convolution fusion | flops 69729792 | bytes 3606528 | tf_op jit(solution)/shard_map/ihd,jd->hij/dot_general | solution.py:520
  76.2 3.8 %fusion = bf16[128,2048]{1,0:T(8,128)(2,1)} fusion(bf16[4,128,2048]{2,1,0:T(8,128)(2,1)} %bitcast.151, bf16[4,128,1024]{2,1,0:T(8,128)(2,1)} %bitcast.152, bf16[4,128,1024]{2,1,0:T(8,128)(2,1)} %get-tuple-element.39, f32[4,128]{1,0:T(4,128)S(1)} %get-tuple-element.38), kind=kOutput, calls=%fused_computation.2 | convolution fusion | flops 403046400 | bytes 4720640 | tf_op jit(solution)/shard_map/hid,hde->ie/dot_general | solution.py:534
  84.0 2.1 %collective-permute-start.10 = (bf16[32,2048]{1,0:T(8,128)(2,1)S(1)}, bf16[32,2048]{1,0:T(8,128)(2,1)S(1)}, u32[]{:S(2)}, u32[]{:S(2)}) collective-permute-start(bf16[32,2048]{1,0:T(8,128)(2,1)S(1)} %slice_bitcast_fusion.10), channel_id=1, source_target_pairs={{0,2},{1,3},{2,0},{3,1},{4,6},{5,7},{6,4},{7,5},{8,10},{9,11},{10,... | collective-permute-start | bytes 393224 | tf_op jit(solution)/shard_map/ppermute | solution.py:423
  86.0 13.6 %collective-permute-done.10 = bf16[32,2048]{1,0:T(8,128)(2,1)S(1)} collective-permute-done((bf16[32,2048]{1,0:T(8,128)(2,1)S(1)}, bf16[32,2048]{1,0:T(8,128)(2,1)S(1)}, u32[]{:S(2)}, u32[]{:S(2)}) %collective-permute-start.10) | collective-permute-done | bytes 131104 | tf_op jit(solution)/shard_map/ppermute | solution.py:423
  99.8 1.6 %add_convert_fusion.2 = (bf16[2,2,32,2048]{3,2,1,0:T(8,128)(2,1)S(1)}, bf16[2,2,32,2048]{3,2,1,0:T(8,128)(2,1)S(1)}) fusion(bf16[2,2,32,2048]{3,2,1,0:T(8,128)(2,1)S(1)} %collective-permute-done.11, bf16[4,4,32,2048]{3,2,1,0:T(8,128)(2,1)} %bitcast.129, bf16[2,2,32,2048]{3,2,1,0:T(8,128)(2,1)S(1)} %collective-permute-done.14), kind=kLoop, calls=%fused_computation.18 | loop fusion | flops 2097152 | bytes 3145728 | tf_op jit(solution)/shard_map/convert_element_type | solution.py:388
  102.4 6.3 %collective-permute-done.12 = bf16[2,32,2048]{2,1,0:T(8,128)(2,1)S(1)} collective-permute-done((bf16[2,32,2048]{2,1,0:T(8,128)(2,1)S(1)}, bf16[2,32,2048]{2,1,0:T(8,128)(2,1)S(1)}, u32[]{:S(2)}, u32[]{:S(2)}) %collective-permute-start.12) | collective-permute-done | bytes 262176 | tf_op jit(solution)/shard_map/ppermute | solution.py:423
  108.8 3.1 %collective-permute-start.13 = (bf16[32,2048]{1,0:T(8,128)(2,1)S(1)}, bf16[32,2048]{1,0:T(8,128)(2,1)S(1)}, u32[]{:S(2)}, u32[]{:S(2)}) collective-permute-start(bf16[32,2048]{1,0:T(8,128)(2,1)S(1)} %slice_bitcast_fusion.8), channel_id=1, source_target_pairs={{0,8},{4,12},{8,0},{12,4},{16,24},{20,28},{24,16},{28,20},{1,9},{5... | collective-permute-start | bytes 393224 | tf_op jit(solution)/shard_map/ppermute | solution.py:423
  112.0 1.7 %collective-permute-start.16 = (bf16[32,2048]{1,0:T(8,128)(2,1)S(1)}, bf16[32,2048]{1,0:T(8,128)(2,1)S(1)}, u32[]{:S(2)}, u32[]{:S(2)}) collective-permute-start(bf16[32,2048]{1,0:T(8,128)(2,1)S(1)} %get-tuple-element.34), channel_id=1, source_target_pairs={{0,16},{4,20},{8,24},{12,28},{16,0},{20,4},{24,8},{28,12},{1,17},{... | collective-permute-start | bytes 393224 | tf_op jit(solution)/shard_map/ppermute | solution.py:423
  116.0 7.2 %collective-permute-done.16 = bf16[32,2048]{1,0:T(8,128)(2,1)S(1)} collective-permute-done((bf16[32,2048]{1,0:T(8,128)(2,1)S(1)}, bf16[32,2048]{1,0:T(8,128)(2,1)S(1)}, u32[]{:S(2)}, u32[]{:S(2)}) %collective-permute-start.16) | collective-permute-done | bytes 131104 | tf_op jit(solution)/shard_map/ppermute | solution.py:423
  (86 shorter events, 27.4 us)
Async XLA Ops:
  0.6 14.4 %copy-start = (bf16[2048,768]{1,0:T(8,128)(2,1)S(1)}, bf16[2048,768]{1,0:T(8,128)(2,1)}, u32[]{:S(2)}) copy-start(bf16[2048,768]{1,0:T(8,128)(2,1)} %param.19) | copy-start | bytes 9437188
  0.7 10.9 %copy-start.7 = (f32[32]{0:T(128)}, f32[32]{0:T(128)S(1)}, u32[]{:S(2)}) copy-start(f32[32]{0:T(128)S(1)} %multiply_power_fusion) | copy-start | bytes 388
  1.9 13.1 %copy-start.5 = (f32[2048]{0:T(1024)S(1)}, f32[2048]{0:T(1024)}, u32[]{:S(2)}) copy-start(f32[2048]{0:T(1024)} %param.18) | copy-start | bytes 24580
  5.9 11.6 %collective-permute-start = (bf16[1,32,2688]{2,1,0:T(8,128)(2,1)}, bf16[1,32,2688]{2,1,0:T(8,128)(2,1)}, u32[]{:S(2)}, u32[]{:S(2)}) collective-permute-start(bf16[1,32,2688]{2,1,0:T(8,128)(2,1)} %bitcast.137), channel_id=1, source_target_pairs={{0,8},{4,12},{8,0},{12,4},{16,24},{20,28},{24,16},{28,20},{1,9},{5... | collective-permute-start | bytes 516104 | tf_op jit(solution)/shard_map/ppermute | solution.py:423
  8.9 15.8 %collective-permute-start.1 = (bf16[1,32,2688]{2,1,0:T(8,128)(2,1)}, bf16[1,32,2688]{2,1,0:T(8,128)(2,1)}, u32[]{:S(2)}, u32[]{:S(2)}) collective-permute-start(bf16[1,32,2688]{2,1,0:T(8,128)(2,1)} %bitcast.138), channel_id=1, source_target_pairs={{0,16},{4,20},{8,24},{12,28},{16,0},{20,4},{24,8},{28,12},{1,17},{... | collective-permute-start | bytes 516104 | tf_op jit(solution)/shard_map/ppermute | solution.py:423
  11.5 13.2 %collective-permute-start.2 = (bf16[1,32,2688]{2,1,0:T(8,128)(2,1)}, bf16[1,32,2688]{2,1,0:T(8,128)(2,1)}, u32[]{:S(2)}, u32[]{:S(2)}) collective-permute-start(bf16[1,32,2688]{2,1,0:T(8,128)(2,1)} %bitcast.139), channel_id=1, source_target_pairs={{0,24},{4,28},{8,16},{12,20},{16,8},{20,12},{24,0},{28,4},{1,25},{... | collective-permute-start | bytes 516104 | tf_op jit(solution)/shard_map/ppermute | solution.py:423
  15.1 9.7 %copy-start.3 = (bf16[32,2688]{1,0:T(8,128)(2,1)S(1)}, bf16[32,2688]{1,0:T(8,128)(2,1)}, u32[]{:S(2)}) copy-start(bf16[32,2688]{1,0:T(8,128)(2,1)} %own_rows.1) | copy-start | bytes 516100
  26.0 14.8 %collective-permute-start.3 = (bf16[4,32,2688]{2,1,0:T(8,128)(2,1)S(1)}, bf16[4,32,2688]{2,1,0:T(8,128)(2,1)S(1)}, u32[]{:S(2)}, u32[]{:S(2)}) collective-permute-start(bf16[4,32,2688]{2,1,0:T(8,128)(2,1)S(1)} %pad_maximum_fusion.1), channel_id=1, source_target_pairs={{0,2},{1,3},{2,0},{3,1},{4,6},{5,7},{6,4},{7,5},{8,10},{9,11},{10,... | collective-permute-start | bytes 2064392 | tf_op jit(solution)/shard_map/ppermute | solution.py:423
  27.6 16.5 %collective-permute-start.4 = (bf16[4,32,2688]{2,1,0:T(8,128)(2,1)S(1)}, bf16[4,32,2688]{2,1,0:T(8,128)(2,1)S(1)}, u32[]{:S(2)}, u32[]{:S(2)}) collective-permute-start(bf16[4,32,2688]{2,1,0:T(8,128)(2,1)S(1)} %pad_maximum_fusion.1), channel_id=1, source_target_pairs={{0,4},{4,0},{8,12},{12,8},{16,20},{20,16},{24,28},{28,24},{1,5},{5... | collective-permute-start | bytes 2064392 | tf_op jit(solution)/shard_map/ppermute | solution.py:423
  40.8 8.6 %collective-permute-start.5 = (bf16[2,32,2688]{2,1,0:T(8,128)(2,1)S(1)}, bf16[2,32,2688]{2,1,0:T(8,128)(2,1)S(1)}, u32[]{:S(2)}, u32[]{:S(2)}) collective-permute-start(bf16[2,32,2688]{2,1,0:T(8,128)(2,1)S(1)} %slice.107), channel_id=1, source_target_pairs={{0,4},{4,0},{8,12},{12,8},{16,20},{20,16},{24,28},{28,24},{1,5},{5... | collective-permute-start | bytes 1032200 | tf_op jit(solution)/shard_map/ppermute | solution.py:423
  44.1 7.3 %collective-permute-start.6 = (bf16[2,32,2688]{2,1,0:T(8,128)(2,1)S(1)}, bf16[2,32,2688]{2,1,0:T(8,128)(2,1)S(1)}, u32[]{:S(2)}, u32[]{:S(2)}) collective-permute-start(bf16[2,32,2688]{2,1,0:T(8,128)(2,1)S(1)} %slice.108), channel_id=1, source_target_pairs={{0,2},{1,3},{2,0},{3,1},{4,6},{5,7},{6,4},{7,5},{8,10},{9,11},{10,... | collective-permute-start | bytes 1032200 | tf_op jit(solution)/shard_map/ppermute | solution.py:423
  52.2 5.4 %collective-permute-start.7 = (bf16[512,2688]{1,0:T(8,128)(2,1)}, bf16[512,2688]{1,0:T(8,128)(2,1)}, u32[]{:S(2)}, u32[]{:S(2)}) collective-permute-start(bf16[512,2688]{1,0:T(8,128)(2,1)} %bitcast.43.refs_1_.refs_2_), channel_id=1, source_target_pairs={{0,1},{1,0},{2,3},{3,2},{4,5},{5,4},{6,7},{7,6},{8,9},{9,8},{10,11... | collective-permute-start | bytes 8257544 | tf_op jit(solution)/shard_map/ppermute | solution.py:423
  63.0 4.6 %collective-permute-start.8 = (bf16[512,2048]{1,0:T(8,128)(2,1)}, bf16[512,2048]{1,0:T(8,128)(2,1)}, u32[]{:S(2)}, u32[]{:S(2)}) collective-permute-start(bf16[512,2048]{1,0:T(8,128)(2,1)} %expert_rows.3), channel_id=1, source_target_pairs={{0,1},{1,0},{2,3},{3,2},{4,5},{5,4},{6,7},{7,6},{8,9},{9,8},{10,11... | collective-permute-start | bytes 6291464 | tf_op jit(solution)/shard_map/ppermute | solution.py:423
  65.0 2.6 %copy-start.2 = (bf16[512,2048]{1,0:T(8,128)(2,1)S(1)}, bf16[512,2048]{1,0:T(8,128)(2,1)}, u32[]{:S(2)}) copy-start(bf16[512,2048]{1,0:T(8,128)(2,1)} %expert_rows.2) | copy-start | bytes 6291460
  81.0 1.9 %collective-permute-start.9 = (bf16[2,32,2048]{2,1,0:T(8,128)(2,1)S(1)}, bf16[2,32,2048]{2,1,0:T(8,128)(2,1)S(1)}, u32[]{:S(2)}, u32[]{:S(2)}) collective-permute-start(bf16[2,32,2048]{2,1,0:T(8,128)(2,1)S(1)} %slice_bitcast_fusion.4), channel_id=1, source_target_pairs={{0,1},{1,0},{2,3},{3,2},{4,5},{5,4},{6,7},{7,6},{8,9},{9,8},{10,11... | collective-permute-start | bytes 786440 | tf_op jit(solution)/shard_map/ppermute | solution.py:423
  81.4 18.4 %collective-permute-start.11 = (bf16[2,2,32,2048]{3,2,1,0:T(8,128)(2,1)}, bf16[2,2,32,2048]{3,2,1,0:T(8,128)(2,1)S(1)}, u32[]{:S(2)}, u32[]{:S(2)}) collective-permute-start(bf16[2,2,32,2048]{3,2,1,0:T(8,128)(2,1)} %get-tuple-element.22), channel_id=1, source_target_pairs={{0,4},{4,0},{8,12},{12,8},{16,20},{20,16},{24,28},{28,24},{1,5},{5... | collective-permute-start | bytes 1572872 | tf_op jit(solution)/shard_map/ppermute | solution.py:423
  82.9 16.9 %collective-permute-start.14 = (bf16[2,2,32,2048]{3,2,1,0:T(8,128)(2,1)}, bf16[2,2,32,2048]{3,2,1,0:T(8,128)(2,1)S(1)}, u32[]{:S(2)}, u32[]{:S(2)}) collective-permute-start(bf16[2,2,32,2048]{3,2,1,0:T(8,128)(2,1)} %get-tuple-element.23), channel_id=1, source_target_pairs={{0,2},{1,3},{2,0},{3,1},{4,6},{5,7},{6,4},{7,5},{8,10},{9,11},{10,... | collective-permute-start | bytes 1572872 | tf_op jit(solution)/shard_map/ppermute | solution.py:423
  84.0 15.7 %collective-permute-start.10 = (bf16[32,2048]{1,0:T(8,128)(2,1)S(1)}, bf16[32,2048]{1,0:T(8,128)(2,1)S(1)}, u32[]{:S(2)}, u32[]{:S(2)}) collective-permute-start(bf16[32,2048]{1,0:T(8,128)(2,1)S(1)} %slice_bitcast_fusion.10), channel_id=1, source_target_pairs={{0,2},{1,3},{2,0},{3,1},{4,6},{5,7},{6,4},{7,5},{8,10},{9,11},{10,... | collective-permute-start | bytes 393224 | tf_op jit(solution)/shard_map/ppermute | solution.py:423
  101.4 13.5 %copy-start.6 = (f32[2048]{0:T(1024)S(1)}, f32[2048]{0:T(1024)}, u32[]{:S(2)}) copy-start(f32[2048]{0:T(1024)} %param.26) | copy-start | bytes 24580
  101.4 7.3 %collective-permute-start.12 = (bf16[2,32,2048]{2,1,0:T(8,128)(2,1)S(1)}, bf16[2,32,2048]{2,1,0:T(8,128)(2,1)S(1)}, u32[]{:S(2)}, u32[]{:S(2)}) collective-permute-start(bf16[2,32,2048]{2,1,0:T(8,128)(2,1)S(1)} %slice_bitcast_fusion.2), channel_id=1, source_target_pairs={{0,2},{1,3},{2,0},{3,1},{4,6},{5,7},{6,4},{7,5},{8,10},{9,11},{10,... | collective-permute-start | bytes 786440 | tf_op jit(solution)/shard_map/ppermute | solution.py:423
  101.8 10.1 %collective-permute-start.15 = (bf16[2,32,2048]{2,1,0:T(8,128)(2,1)S(1)}, bf16[2,32,2048]{2,1,0:T(8,128)(2,1)S(1)}, u32[]{:S(2)}, u32[]{:S(2)}) collective-permute-start(bf16[2,32,2048]{2,1,0:T(8,128)(2,1)S(1)} %slice_bitcast_fusion), channel_id=1, source_target_pairs={{0,4},{4,0},{8,12},{12,8},{16,20},{20,16},{24,28},{28,24},{1,5},{5... | collective-permute-start | bytes 786440 | tf_op jit(solution)/shard_map/ppermute | solution.py:423
  108.8 7.2 %collective-permute-start.13 = (bf16[32,2048]{1,0:T(8,128)(2,1)S(1)}, bf16[32,2048]{1,0:T(8,128)(2,1)S(1)}, u32[]{:S(2)}, u32[]{:S(2)}) collective-permute-start(bf16[32,2048]{1,0:T(8,128)(2,1)S(1)} %slice_bitcast_fusion.8), channel_id=1, source_target_pairs={{0,8},{4,12},{8,0},{12,4},{16,24},{20,28},{24,16},{28,20},{1,9},{5... | collective-permute-start | bytes 393224 | tf_op jit(solution)/shard_map/ppermute | solution.py:423
  112.0 11.2 %collective-permute-start.16 = (bf16[32,2048]{1,0:T(8,128)(2,1)S(1)}, bf16[32,2048]{1,0:T(8,128)(2,1)S(1)}, u32[]{:S(2)}, u32[]{:S(2)}) collective-permute-start(bf16[32,2048]{1,0:T(8,128)(2,1)S(1)} %get-tuple-element.34), channel_id=1, source_target_pairs={{0,16},{4,20},{8,24},{12,28},{16,0},{20,4},{24,8},{28,12},{1,17},{... | collective-permute-start | bytes 393224 | tf_op jit(solution)/shard_map/ppermute | solution.py:423
  113.7 9.5 %collective-permute-start.17 = (bf16[32,2048]{1,0:T(8,128)(2,1)S(1)}, bf16[32,2048]{1,0:T(8,128)(2,1)S(1)}, u32[]{:S(2)}, u32[]{:S(2)}) collective-permute-start(bf16[32,2048]{1,0:T(8,128)(2,1)S(1)} %get-tuple-element.35), channel_id=1, source_target_pairs={{0,24},{4,28},{8,16},{12,20},{16,8},{20,12},{24,0},{28,4},{1,25},{... | collective-permute-start | bytes 393224 | tf_op jit(solution)/shard_map/ppermute | solution.py:423
  (4 other events, 6.5 us)
